TPU v7x, 512 devices: a whole 4x8x8 slice. The times are simulated.
512 devices in a mesh: ep: 32 (over z, x), tp: 16 (over y, core).
Axes of the slice: x: 4, y: 8, z: 8, core: 2. Of those that a mesh axis runs over, the one named last changes fastest.
Arguments:
- x_in: bfloat16 [4096, 12288], P('tp', 'ep'), may hold values from -6 to 6
- z_in: bfloat16 [4096, 12288], P('tp', 'ep'), may hold values from -6 to 6
- dt_raw: float32 [64, 12288], P('tp', 'ep'), may hold values from -6 to 6
- decay_rate: float32 [64], P('tp'), may hold values from 0 to 1, as said below
- b_in: bfloat16 [256, 12288], P(None, 'ep'), may hold values from -6 to 6
- c_in: bfloat16 [256, 12288], P(None, 'ep'), may hold values from -6 to 6
- conv_x: float32 [4096, 4], P('tp'), may hold values from -3 to 3
- conv_b: float32 [256, 4], replicated, may hold values from -3 to 3
- conv_c: float32 [256, 4], replicated, may hold values from -3 to 3
- head_gain: float32 [4096], P('tp'), may hold values from 0.1 to 1.9
- moe_rows: bfloat16 [5120, 2048], P('ep'), may hold values from -6 to 6
- moe_gain: float32 [2048], replicated, may hold values from 0.1 to 1.9
- routes: int32 [5120, 2], P('ep'), may hold values from 0 to 31, all different within a row; in each aligned block of 160 rows (0 to 159, 160 to 319, ...) at most 20 rows name the same one
- route_logit: float32 [5120, 2], P('ep'), may hold values from -6 to 6
- w_gate: bfloat16 [32, 2048, 5120], P('ep', None, 'tp'), may hold values from -0.125 to 0.125
- w_up: bfloat16 [32, 2048, 5120], P('ep', None, 'tp'), may hold values from -0.125 to 0.125
- w_down: bfloat16 [32, 5120, 2048], P('ep', 'tp'), may hold values from -0.078125 to 0.078125
Outputs:
- mixed: bfloat16 [4096, 12288], P('tp', 'ep')
- moe_out: bfloat16 [2048, 5120], P('tp', 'ep')
Inputs may be any that keep to these rules, and one draw needn't show every extreme that they name: `routes`: each row names 2 different experts; among the rows of one index of ep no expert is named more than 20 times, a bound that some block reaches. `decay_rate`: positive rates.
All inputs are finite; a program needn't handle non-finite values.
Results may differ from a plain program's by a relative error of at most 0.018.
Values may be sent and summed in bfloat16 or wider, within the bound.
A program may use at most 64 MiB of HBM per device.

v0:
```python
import functools
import jax
import jax.numpy as jnp
from jax import lax
from jax.experimental import pallas as pl
from jax.experimental.pallas import tpu as pltpu
from jax.sharding import PartitionSpec as P

HEADS = 64
HEAD_DIM = 64
GROUPS = 2
NSTATE = 128
BLOCK = 128
ROW_EPS = 0.1
HEAD_EPS = 1.0
LANES = 128
F32 = jnp.float32
BF16 = jnp.bfloat16
VMEM = pltpu.VMEM
MESH = pl.DeviceIdType.MESH


def vmem_specs(count):
    return [pl.BlockSpec(memory_space=VMEM)] * count


def cost(flops, moved):
    return pl.CostEstimate(flops=flops, bytes_accessed=moved, transcendentals=0)


def dot(a, b, dims, precision=None):
    return lax.dot_general(a, b, (dims, ((), ())), preferred_element_type=F32, precision=precision)


def eye(count):
    row = lax.broadcasted_iota(jnp.int32, (count, count), 0)
    col = lax.broadcasted_iota(jnp.int32, (count, count), 1)
    return jnp.where(row == col, 1.0, 0.0).astype(F32)


def upright(flat):
    return dot(flat, eye(flat.shape[0]), ((0,), (0,)), lax.Precision.HIGHEST)


def silu(v):
    return v / (1.0 + jnp.exp(-v))


def conv_rows(signal, rim, weight):
    taps = weight.shape[1]
    joined = jnp.concatenate([rim.astype(F32), signal.astype(F32)], axis=1)
    running = weight[:, taps - 1 : taps] * joined[:, LANES:]
    for back in range(1, taps):
        moved = pltpu.roll(joined, back, 1)[:, LANES:]
        running = running + weight[:, taps - 1 - back : taps - back] * moved
    return silu(running)


def prefix_decays(dt_ref, rate_ref):
    dt = dt_ref[...]
    step = jnp.maximum(dt, 0.0) + jnp.log1p(jnp.exp(-jnp.abs(dt)))
    rate = jnp.where(eye(dt.shape[0]) > 0.0, rate_ref[...], 0.0)
    log_decay = -step * jnp.sum(rate, axis=1, keepdims=True)
    length = dt.shape[1]
    row = lax.broadcasted_iota(jnp.int32, (length, length), 0)
    col = lax.broadcasted_iota(jnp.int32, (length, length), 1)
    upper = jnp.where(row <= col, 1.0, 0.0).astype(F32)
    lower = jnp.where(row >= col, 1.0, 0.0).astype(F32)
    high = lax.Precision.HIGHEST
    cum = dot(log_decay, upper, ((1,), (0,)), high)
    cum_col = dot(lower, log_decay, ((1,), (1,)), high)
    return step, cum, cum_col


def flip(place, mask):
    bit = 1
    while bit <= mask:
        if mask & bit:
            place = place + bit * (1 - 2 * ((place // bit) % 2))
        bit *= 2
    return place


def greet(ep_size, tp_size):
    barrier = pltpu.get_barrier_semaphore()
    me, lane = lax.axis_index("ep"), lax.axis_index("tp")
    count = 0
    for hop in range(1, ep_size):
        pl.semaphore_signal(barrier, 1, device_id={"ep": (me + hop) % ep_size}, device_id_type=MESH)
        count += 1
    bit = 1
    while bit < tp_size:
        pl.semaphore_signal(barrier, 1, device_id={"tp": flip(lane, bit)}, device_id_type=MESH)
        count += 1
        bit *= 2
    pl.semaphore_wait(barrier, count)


def remote(source, target, send, recv, **where):
    return pltpu.make_async_remote_copy(
        src_ref=source, dst_ref=target, send_sem=send, recv_sem=recv, device_id=where, device_id_type=MESH
    )


class Prefix:
    def __init__(self, state, reach, out, out_reach, got, got_reach, send, recv, ep_size):
        self.state, self.reach = state, reach
        self.out, self.out_reach, self.got, self.got_reach = out, out_reach, got, got_reach
        self.send, self.recv, self.size = send, recv, ep_size

    def copies(self, turn, steps):
        target = (lax.axis_index("ep") + steps) % self.size
        return (
            remote(self.out.at[turn], self.got.at[turn], self.send.at[turn, 0], self.recv.at[turn, 0], ep=target),
            remote(self.out_reach.at[turn], self.got_reach.at[turn], self.send.at[turn, 1], self.recv.at[turn, 1], ep=target),
        )

    def begin(self, turn, steps):
        me = lax.axis_index("ep")

        @pl.when(me + steps < self.size)
        def _():
            self.out[turn] = self.state[...].astype(BF16)
            self.out_reach[turn] = self.reach[...]
            for copy in self.copies(turn, steps):
                copy.start()

    def finish(self, turn, steps, first):
        me = lax.axis_index("ep")

        @pl.when(me >= steps)
        def _():
            for copy in self.copies(turn, steps):
                copy.wait_recv()
            if first:
                self.state[...] = self.got[turn].astype(F32)
                self.reach[...] = self.got_reach[turn]
            else:
                for head in range(self.reach.shape[0]):
                    rows = slice(head * HEAD_DIM, (head + 1) * HEAD_DIM)
                    before = self.got[turn, rows, :].astype(F32)
                    self.state[rows, :] = self.state[rows, :] + self.reach[head : head + 1, :] * before
                self.reach[...] = self.reach[...] * self.got_reach[turn]

        if first:

            @pl.when(me < steps)
            def _():
                self.state[...] = jnp.zeros_like(self.state)
                self.reach[...] = jnp.zeros_like(self.reach)

        @pl.when(me + steps < self.size)
        def _():
            for copy in self.copies(turn, steps):
                copy.wait_send()


def spread_kernel(
    rows_ref, gain_ref, routes_ref, logit_ref, x_ref, tapx_ref, b_ref, tapb_ref, c_ref, tapc_ref, dt_ref, rate_ref,
    joined_ref, pick_ref, y_ref, state_ref, reach_ref, conv_ref, cum_ref,
    outbox, rank_ref, weight_ref, xrim, brim, crim, tap_col, tapb_col, tapc_col,
    step_ref, col_ref, score_ref, bconv_ref, out, out_reach, got, got_reach,
    rim_send, rim_recv, box_send, box_recv, ag_send, ag_recv, pre_send, pre_recv,
    *, ep_size, tp_size,
):
    me, lane = lax.axis_index("ep"), lax.axis_index("tp")
    experts, capacity, features = joined_ref.shape
    width = features // tp_size
    tokens = rows_ref.shape[0]
    heads, length = dt_ref.shape

    def cols(part):
        return pl.ds(pl.multiple_of(flip(lane, part) * width, LANES), width)

    greet(ep_size, tp_size)
    end = pl.ds(length - LANES, LANES)
    after = (me + 1) % ep_size
    rims = [
        remote(source.at[:, end], target, rim_send.at[i], rim_recv.at[i], ep=after)
        for i, (source, target) in enumerate(((x_ref, xrim), (b_ref, brim), (c_ref, crim)))
    ]

    @pl.when(me + 1 < ep_size)
    def _():
        for copy in rims:
            copy.start()

    @pl.when(me == 0)
    def _():
        for ref in (xrim, brim, crim):
            ref[...] = jnp.zeros_like(ref)

    values = rows_ref[...].astype(F32)
    scale = lax.rsqrt(jnp.mean(values * values, axis=1, keepdims=True) + ROW_EPS)
    normed = (rows_ref[:, cols(0)].astype(F32) * scale * gain_ref[:, cols(0)]).astype(BF16)
    routes = routes_ref[...]
    logit = logit_ref[...]
    first = 1.0 / (1.0 + jnp.exp(logit[1:2] - logit[0:1]))
    second = 1.0 / (1.0 + jnp.exp(logit[0:1] - logit[1:2]))
    number = lax.broadcasted_iota(jnp.int32, (experts, tokens), 0)
    in_first = number == routes[0:1]
    in_second = number == routes[1:2]
    hits = jnp.where(in_first, 1.0, 0.0) + jnp.where(in_second, 1.0, 0.0)
    row = lax.broadcasted_iota(jnp.int32, (tokens, tokens), 0)
    col = lax.broadcasted_iota(jnp.int32, (tokens, tokens), 1)
    earlier = jnp.where(row < col, 1.0, 0.0).astype(BF16)
    rank = dot(hits.astype(BF16), earlier, ((1,), (0,)))
    weight_ref[...] = jnp.where(in_first, first, 0.0) + jnp.where(in_second, second, 0.0)
    rank_ref[...] = jnp.where(hits > 0.0, rank, -1.0)
    place = lax.broadcasted_iota(jnp.int32, (capacity, tokens), 0).astype(F32)

    def box(hop):
        return remote(
            outbox.at[hop], joined_ref.at[me, :, cols(0)], box_send.at[hop], box_recv.at[hop], ep=(me + hop) % ep_size
        )

    for hop in list(range(1, ep_size)) + [0]:
        expert = (me + hop) % ep_size
        same = place == rank_ref[pl.ds(expert, 1), :]
        pick_ref[expert] = jnp.where(same, weight_ref[pl.ds(expert, 1), :], 0.0).astype(BF16)
        chosen = dot(jnp.where(same, 1.0, 0.0).astype(BF16), normed, ((1,), (0,))).astype(BF16)
        if hop:
            outbox[hop] = chosen
            box(hop).start()
        else:
            joined_ref[me, :, cols(0)] = chosen

    def passing(part, bit, hop):
        at = joined_ref.at[(me + ep_size - hop) % ep_size, :, cols(part)]
        return remote(at, at, ag_send.at[part + bit, hop], ag_recv.at[part + bit, hop], tp=flip(lane, bit))

    bits = [1 << i for i in range(tp_size.bit_length() - 1)][::-1]
    passing(0, bits[0], 0).start()

    tap_col[...] = upright(tapx_ref[...])
    tapb_col[...] = upright(tapb_ref[...])
    tapc_col[...] = upright(tapc_ref[...])
    step, cum, cum_col = prefix_decays(dt_ref, rate_ref)
    step_ref[...] = step
    cum_ref[...] = cum
    reach_ref[...] = jnp.broadcast_to(jnp.exp(cum[:, length - 1 :]), reach_ref.shape)
    for head in range(heads):
        col_ref[head] = jnp.broadcast_to(cum_col[:, head : head + 1], (length, LANES))

    @pl.when(me > 0)
    def _():
        for copy in rims:
            copy.wait_recv()

    group = pl.ds(pl.multiple_of(lane * heads // (HEADS // GROUPS) * NSTATE, NSTATE), NSTATE)
    b_conv = conv_rows(b_ref[group, :], brim[group, :], tapb_col[group, :]).astype(BF16)
    c_conv = conv_rows(c_ref[group, :], crim[group, :], tapc_col[group, :]).astype(BF16)
    bconv_ref[...] = b_conv
    conv_ref[...] = c_conv
    score_ref[...] = dot(b_conv, c_conv, ((0,), (0,)))
    brow = lax.broadcasted_iota(jnp.int32, (BLOCK, BLOCK), 0)
    bcol = lax.broadcasted_iota(jnp.int32, (BLOCK, BLOCK), 1)
    causal = brow <= bcol

    def one(head, carry):
        rows = pl.ds(pl.multiple_of(head * HEAD_DIM, HEAD_DIM), HEAD_DIM)
        x = conv_rows(x_ref[rows, :], xrim[rows, :], tap_col[rows, :])
        own = cum_ref[pl.ds(head, 1), :]
        xs = x * step_ref[pl.ds(head, 1), :]
        tail = xs * jnp.exp(own[:, length - 1 :] - own)
        state_ref[rows, :] = dot(tail.astype(BF16), bconv_ref[...], ((1,), (1,)))
        xs = xs.astype(BF16)
        for target in range(length // BLOCK):
            at = slice(target * BLOCK, (target + 1) * BLOCK)
            pieces = []
            for source in range(target + 1):
                of = slice(source * BLOCK, (source + 1) * BLOCK)
                gap = own[:, at] - col_ref[head, of, :]
                if source == target:
                    gap = jnp.where(causal, gap, -jnp.inf)
                pieces.append((score_ref[of, at] * jnp.exp(gap)).astype(BF16))
            mask = pieces[0] if target == 0 else jnp.concatenate(pieces, axis=0)
            y_ref[rows, at] = dot(xs[:, : (target + 1) * BLOCK], mask, ((1,), (0,)))
        return carry

    lax.fori_loop(0, heads * 3 // 4, one, 0)
    for hop in range(1, ep_size):
        if hop == ep_size // 2:
            lax.fori_loop(heads * 3 // 4, heads, one, 0)
            chain = Prefix(
                state_ref, reach_ref, out, out_reach, got, got_reach, pre_send, pre_recv, ep_size
            )
            chain.begin(0, 1)
        box(hop).wait_recv()
        passing(0, bits[0], hop).start()
    have = [0]
    for index, bit in enumerate(bits):
        for hop in range(ep_size):
            passing(0, bit, hop).wait_recv()
            for part in have[1:]:
                passing(part, bit, hop).wait_recv()
            if index + 1 < len(bits):
                for part in have + [part + bit for part in have]:
                    passing(part, bits[index + 1], hop).start()
        have = have + [part + bit for part in have]
        if index == 0:
            chain.finish(0, 1, True)
            chain.begin(1, 1)
    chain.finish(1, 1, False)
    have = [0]
    for bit in bits:
        for hop in range(ep_size):
            for part in have:
                passing(part, bit, hop).wait_send()
        have = have + [part + bit for part in have]
    for hop in range(1, ep_size):
        box(hop).wait_send()

    @pl.when(me + 1 < ep_size)
    def _():
        for copy in rims:
            copy.wait_send()


def gather_kernel(
    part_ref, first_ref, first_reach,
    back_ref, state_ref,
    sums, landed, final, reach_ref, out, out_reach, got, got_reach,
    rs_send, rs_recv, box_send, box_recv, pre_send, pre_recv,
    *, ep_size, tp_size, rounds,
):
    me, lane = lax.axis_index("ep"), lax.axis_index("tp")
    width = part_ref.shape[2] // tp_size
    greet(ep_size, tp_size)
    bits = [1 << i for i in range(tp_size.bit_length() - 1)]
    order = list(range(1, ep_size)) + [0]

    def cols(part):
        return pl.ds(pl.multiple_of(flip(lane, part) * width, LANES), width)

    def passing(part, bit, hop):
        chunk = (me + hop) % ep_size
        source = part_ref.at[chunk, :, cols(part)] if bit == 1 else sums.at[part, chunk]
        return remote(source, landed.at[part, chunk], rs_send.at[part, hop], rs_recv.at[part, hop], tp=flip(lane, bit))

    def box(hop):
        return remote(final.at[hop], back_ref.at[me], box_send.at[hop], box_recv.at[hop], ep=(me + hop) % ep_size)

    for hop in order:
        for part in range(1, tp_size, 2):
            passing(part, 1, hop).start()
    state_ref[...] = first_ref[...]
    reach_ref[...] = first_reach[...]
    chain = Prefix(state_ref, reach_ref, out, out_reach, got, got_reach, pre_send, pre_recv, ep_size)
    if rounds:
        chain.begin(0, rounds[0])
    done = 0
    for bit in bits:
        kept = range(0, tp_size, 2 * bit)
        for hop in order:
            chunk = (me + hop) % ep_size
            for part in list(kept)[::-1]:
                passing(part + bit, bit, hop).wait_recv()
                mine = part_ref[chunk, :, cols(part)] if bit == 1 else sums[part, chunk]
                total = (mine.astype(F32) + landed[part + bit, chunk].astype(F32)).astype(BF16)
                if bit < bits[-1]:
                    sums[part, chunk] = total
                    if part & (2 * bit):
                        passing(part, 2 * bit, hop).start()
                elif hop:
                    final[hop] = total
                    box(hop).start()
                else:
                    back_ref[me] = total
        if done < len(rounds):
            chain.finish(done, rounds[done], False)
            done += 1
            if done < len(rounds):
                chain.begin(done, rounds[done])
    while done < len(rounds):
        chain.finish(done, rounds[done], False)
        done += 1
        if done < len(rounds):
            chain.begin(done, rounds[done])
    for hop in range(1, ep_size):
        box(hop).wait_recv()
        box(hop).wait_send()
    for bit in bits:
        for part in range(bit, tp_size, 2 * bit):
            for hop in order:
                passing(part, bit, hop).wait_send()


def close_kernel(y_ref, state_ref, conv_ref, cum_ref, z_ref, gain_ref, out_ref, gain_col):
    heads = cum_ref.shape[0]
    top = lax.broadcasted_iota(jnp.int32, (8, LANES), 0) == 0
    flat = jnp.broadcast_to(gain_ref[...], (8, gain_ref.shape[1]))
    gain_col[...] = dot(flat, jnp.where(top, 1.0, 0.0), ((0,), (0,)), lax.Precision.HIGHEST)

    def one(head, carry):
        rows = pl.ds(pl.multiple_of(head * HEAD_DIM, HEAD_DIM), HEAD_DIM)
        carried = dot(state_ref[rows, :].astype(BF16), conv_ref[...], ((1,), (0,)))
        y = y_ref[rows, :] + carried * jnp.exp(cum_ref[pl.ds(head, 1), :])
        gated = y * silu(z_ref[rows, :].astype(F32))
        scale = lax.rsqrt(jnp.mean(gated * gated, axis=0, keepdims=True) + HEAD_EPS)
        out_ref[rows, :] = (gated * scale * gain_col[rows, 0:1]).astype(BF16)
        return carry

    lax.fori_loop(0, heads, one, 0)


def ffn_kernel(joined, gate_ref, up_ref, down_ref, out_ref, total):
    turn = pl.program_id(0)
    gate = dot(joined[...], gate_ref[0], ((1,), (0,)))
    up = dot(joined[...], up_ref[0], ((1,), (0,)))
    hidden = (silu(gate) * up).astype(BF16)
    partial = dot(hidden, down_ref[0], ((1,), (0,)))

    @pl.when(turn == 0)
    def _():
        total[...] = partial

    @pl.when(turn > 0)
    def _():
        total[...] += partial

    @pl.when(turn == pl.num_programs(0) - 1)
    def _():
        out_ref[...] = total[...].astype(BF16)


def combine_kernel(back_ref, pick_ref, out_ref):
    out_ref[...] = dot(pick_ref[...], back_ref[...], ((0,), (0,))).astype(BF16)


def on_device(
    x_in, z_in, dt_raw, decay_rate, b_in, c_in, conv_x, conv_b, conv_c, head_gain,
    moe_rows, moe_gain, routes, route_logit, w_gate, w_up, w_down,
):
    heads, length = dt_raw.shape
    value_rows = x_in.shape[0]
    taps = conv_x.shape[1]
    tp_size = lax.axis_size("tp")
    ep_size = lax.axis_size("ep")
    tokens, features = moe_rows.shape
    experts = ep_size
    capacity = 2 * tokens * routes.shape[1] // experts
    width = features // tp_size
    slots = experts * capacity
    dma = pltpu.SemaphoreType.DMA
    shape = jax.ShapeDtypeStruct

    def chain(turns):
        return [
            VMEM((turns, value_rows, NSTATE), BF16),
            VMEM((turns, heads, NSTATE), F32),
            VMEM((turns, value_rows, NSTATE), BF16),
            VMEM((turns, heads, NSTATE), F32),
        ]

    joined, pick, y_local, state, reach, c_conv, cum = pl.pallas_call(
        functools.partial(spread_kernel, ep_size=ep_size, tp_size=tp_size),
        out_shape=(
            shape((experts, capacity, features), BF16),
            shape((experts, capacity, tokens), BF16),
            shape((value_rows, length), F32),
            shape((value_rows, NSTATE), F32),
            shape((heads, NSTATE), F32),
            shape((NSTATE, length), BF16),
            shape((heads, length), F32),
        ),
        in_specs=vmem_specs(12),
        out_specs=tuple(vmem_specs(7)),
        scratch_shapes=[
            VMEM((experts, capacity, width), BF16),
            VMEM((experts, tokens), F32),
            VMEM((experts, tokens), F32),
            VMEM((value_rows, LANES), BF16),
            VMEM((b_in.shape[0], LANES), BF16),
            VMEM((c_in.shape[0], LANES), BF16),
            VMEM((value_rows, taps), F32),
            VMEM((b_in.shape[0], taps), F32),
            VMEM((c_in.shape[0], taps), F32),
            VMEM((heads, length), F32),
            VMEM((heads, length, LANES), F32),
            VMEM((length, length), F32),
            VMEM((NSTATE, length), BF16),
        ]
        + chain(2)
        + [
            dma((3,)), dma((3,)), dma((ep_size,)), dma((ep_size,)),
            dma((tp_size, ep_size)), dma((tp_size, ep_size)), dma((2, 2)), dma((2, 2)),
        ],
        compiler_params=pltpu.CompilerParams(collective_id=0, has_side_effects=True, vmem_limit_bytes=48 * 2**20),
        name="spread",
    )(
        moe_rows, moe_gain.reshape(1, features), routes.T, route_logit.T,
        x_in, conv_x.T, b_in, conv_b.T, c_in, conv_c.T, dt_raw, decay_rate.reshape(1, heads),
    )

    hidden_units = w_gate.shape[2]
    tile = hidden_units if hidden_units < 1024 else 256
    partial = pl.pallas_call(
        ffn_kernel,
        grid=(hidden_units // tile,),
        out_shape=shape((slots, features), BF16),
        in_specs=vmem_specs(1)
        + [
            pl.BlockSpec((1, features, tile), lambda i: (0, 0, i)),
            pl.BlockSpec((1, features, tile), lambda i: (0, 0, i)),
            pl.BlockSpec((1, tile, features), lambda i: (0, i, 0)),
        ],
        out_specs=pl.BlockSpec(memory_space=VMEM),
        scratch_shapes=[VMEM((slots, features), F32)],
        compiler_params=pltpu.CompilerParams(dimension_semantics=("arbitrary",), vmem_limit_bytes=48 * 2**20),
        name="ffn",
    )(joined.reshape(slots, features), w_gate, w_up, w_down)

    rounds = []
    steps = 2
    while steps < ep_size - 1:
        rounds.append(steps)
        steps *= 2
    turns = max(1, len(rounds))
    returned, incoming = pl.pallas_call(
        functools.partial(gather_kernel, ep_size=ep_size, tp_size=tp_size, rounds=rounds),
        out_shape=(shape((experts, capacity, width), BF16), shape((value_rows, NSTATE), F32)),
        in_specs=vmem_specs(3),
        out_specs=tuple(vmem_specs(2)),
        scratch_shapes=[
            VMEM((tp_size, experts, capacity, width), BF16),
            VMEM((tp_size, experts, capacity, width), BF16),
            VMEM((experts, capacity, width), BF16),
            VMEM((heads, NSTATE), F32),
        ]
        + chain(turns)
        + [
            dma((tp_size, ep_size)), dma((tp_size, ep_size)), dma((ep_size,)), dma((ep_size,)),
            dma((turns, 2)), dma((turns, 2)),
        ],
        compiler_params=pltpu.CompilerParams(collective_id=1, has_side_effects=True, vmem_limit_bytes=48 * 2**20),
        name="gather",
    )(partial.reshape(experts, capacity, features), state, reach)

    mixed = pl.pallas_call(
        close_kernel,
        out_shape=shape((value_rows, length), BF16),
        in_specs=vmem_specs(6),
        out_specs=pl.BlockSpec(memory_space=VMEM),
        scratch_shapes=[VMEM((value_rows, LANES), F32)],
        name="close",
    )(y_local, incoming, c_conv, cum, z_in, head_gain.reshape(1, value_rows))
    moe_out = pl.pallas_call(
        combine_kernel,
        out_shape=shape((tokens, width), BF16),
        in_specs=vmem_specs(2),
        out_specs=pl.BlockSpec(memory_space=VMEM),
        name="combine",
    )(returned.reshape(slots, width), pick.reshape(slots, tokens))
    return (mixed, moe_out.T)


def solution(mesh):
    return jax.shard_map(
        on_device,
        mesh=mesh,
        in_specs=(
            P("tp", "ep"), P("tp", "ep"), P("tp", "ep"), P("tp"), P(None, "ep"), P(None, "ep"),
            P("tp", None), P(), P(), P("tp"), P("ep", None), P(), P("ep", None), P("ep", None),
            P("ep", None, "tp"), P("ep", None, "tp"), P("ep", "tp", None),
        ),
        out_specs=(P("tp", "ep"), P("tp", "ep")),
        check_vma=False,
    )
```

profile of v0, /device:TPU:8, one launch (start us, length us, event | category | flops | bytes accessed | tf_op | source)
XLA Modules:
  0.0 175.8 jit_solution(17058406943050761155)
XLA Ops:
  0.6 0.0 copy-start.1
  0.6 1.1 copy-done.1
  1.7 0.0 copy-start.3
  1.7 0.9 copy-done.3
  2.7 0.0 copy-start.4
  2.7 0.9 copy-done.4
  3.6 0.0 copy-start.5
  3.6 0.9 copy-done.5
  4.5 0.0 copy-start.11
  4.5 0.7 copy-done.11
  5.2 0.0 copy-start.12
  5.2 0.7 copy-done.12
  5.9 0.0 copy-start.14
  5.9 0.7 copy-done.14
  6.6 0.0 copy-start.15
  6.6 0.7 copy-done.15
  7.3 0.0 copy-start.16
  7.3 0.7 copy-done.16
  8.0 0.0 copy-start.17
  8.0 0.7 copy-done.17
  8.6 0.0 copy-start.18
  8.6 0.7 copy-done.18
  9.3 0.0 copy-start.19
  9.3 0.7 copy-done.19
  10.0 71.1 %spread.1 = (bf16[32,20,2048]{2,1,0:T(8,128)(2,1)S(1)}, bf16[32,20,160]{2,1,0:T(8,128)(2,1)S(1)}, f32[256,384]{1,0:T(8,128)S(1)}, f32[256,128]{1,0:T(8,128)S(1)}...) custom-call(bf16[160,2048]{1,0:T(8,128)(2,1)S(1)} %copy-done.1, f32[1,2048]{1,0:T(1,128)S(1)} %bitcast.9, ...), custom_call_target="tpu_custom_call" | custom-call | tf_op jit(solution)/shard_map/spread/pallas_call | solution.py:456
  81.1 0.0 copy-start.2
  81.1 0.8 copy-done.2
  81.9 0.0 copy-start.7
  81.9 0.7 copy-done.7
  82.5 0.0 copy-start.10
  82.5 0.6 copy-done.10
  83.2 0.0 copy-start.13
  83.2 0.6 copy-done.13
  83.8 2.2 %reshape.27.joined = bf16[640,2048]{1,0:T(8,128)(2,1)} reshape(bf16[32,20,2048]{2,1,0:T(8,128)(2,1)S(1)} %get-tuple-element.12) | data formatting | bytes 5242880 | tf_op jit(solution)/shard_map/reshape | solution.py:512
  86.0 1.8 %copy.21.gate_ref = bf16[1,2048,320]{2,1,0:T(8,128)(2,1)S(1)} copy(bf16[1,2048,320]{1,2,0:T(8,128)(2,1)} %param.31) | data formatting | bytes 2621440 | tf_op args[14]
  87.8 1.8 %copy.22.up_ref = bf16[1,2048,320]{2,1,0:T(8,128)(2,1)S(1)} copy(bf16[1,2048,320]{1,2,0:T(8,128)(2,1)} %param.32) | data formatting | bytes 2621440 | tf_op args[15]
  89.6 0.0 copy-start
  89.6 1.3 copy-done
  90.9 7.5 %ffn.1 = bf16[640,2048]{1,0:T(8,128)(2,1)} custom-call(bf16[640,2048]{1,0:T(8,128)(2,1)} %reshape.27.joined, bf16[1,2048,320]{2,1,0:T(8,128)(2,1)S(1)} %copy.21.gate_ref, bf16[1,2048,320]{2,1,0:T(8,128)(2,1)S(1)} %copy.22.up_ref, bf16[1,320,2048]{2,1,0:T(8,128)(2,1)S(1)} %copy-done), custom_call_target="tpu_custom_call" | custom-call | tf_op jit(solution)/shard_map/ffn/pallas_call | solution.py:498
  98.5 3.5 %reshape.28.part_ref = bf16[32,20,2048]{2,1,0:T(8,128)(2,1)S(1)} reshape(bf16[640,2048]{1,0:T(8,128)(2,1)} %ffn.1) | data formatting | bytes 5242880 | tf_op jit(solution)/shard_map/reshape | solution.py:538
  102.0 0.0 copy-start.8
  102.0 0.9 copy-done.8
  102.9 64.3 %gather.1 = (bf16[32,20,128]{2,1,0:T(8,128)(2,1)S(1)}, f32[256,128]{1,0:T(8,128)S(1)}) custom-call(bf16[32,20,2048]{2,1,0:T(8,128)(2,1)S(1)} %reshape.28.part_ref, f32[256,128]{1,0:T(8,128)S(1)} %copy-done.8, f32[4,128]{1,0:T(4,128)S(1)} %get-tuple-element.14.first_reach), custom_call_target="tpu_custom_call" | custom-call | tf_op jit(solution)/shard_map/gather/pallas_call | solution.py:520
  167.2 0.0 copy-start.6
  167.2 0.7 copy-done.6
  167.8 0.0 copy-start.9
  167.8 0.6 copy-done.9
  168.5 2.9 %close.1 = bf16[256,384]{1,0:T(8,128)(2,1)} custom-call(f32[256,384]{1,0:T(8,128)} %copy-done.2, f32[256,128]{1,0:T(8,128)} %copy-done.9, bf16[128,384]{1,0:T(8,128)(2,1)} %copy-done.10, f32[4,384]{1,0:T(4,128)} %copy-done.13, bf16[256,384]{1,0:T(8,128)(2,1)} %z_ref.1, f32[1,256]{1,0:T(1,128)} %bitcast.17), custom_call_target="tpu_custom_call" | custom-call | tf_op jit(solution)/shard_map/close/pallas_call | solution.py:540
  171.4 1.6 reshape.30.back_ref
  173.0 0.9 reshape.31.pick_ref
  173.9 1.9 %combine.1 = bf16[160,128]{1,0:T(8,128)(2,1)} custom-call(bf16[640,128]{1,0:T(8,128)(2,1)} %reshape.30.back_ref, bf16[640,160]{1,0:T(8,128)(2,1)} %reshape.31.pick_ref), custom_call_target="tpu_custom_call" | custom-call | tf_op jit(solution)/shard_map/combine/pallas_call | solution.py:548
Async XLA Ops:
  0.6 1.1 copy-start.1
  1.7 0.9 copy-start.3
  2.7 0.9 copy-start.4
  3.6 0.9 copy-start.5
  4.5 0.7 copy-start.11
  5.2 0.7 copy-start.12
  5.9 0.7 copy-start.14
  6.6 0.7 copy-start.15
  7.3 0.7 copy-start.16
  8.0 0.7 copy-start.17
  8.6 0.7 copy-start.18
  9.3 0.7 copy-start.19
  81.1 0.8 copy-start.2
  81.9 0.7 copy-start.7
  82.5 0.6 copy-start.10
  83.2 0.6 copy-start.13
  89.6 1.3 copy-start
  102.0 0.9 copy-start.8
  167.2 0.7 copy-start.6
  167.8 0.7 copy-start.9
where the time goes:
time: 177 us; the launch traced here: 176 us
  Pallas kernels  148 us (84%)
  local copies, waits for them, and re-layouts  27.3 us (15%)
    pallas_call x1, Pallas kernels, on_device(): pl.pallas_call(functools.partial(spread_kernel, ep_size=ep_size, tp_size=...  71.1 us
    pallas_call x1, Pallas kernels, on_device(): pl.pallas_call(functools.partial(gather_kernel, ep_size=ep_size, tp_size=...  64.3 us
    unnamed x42, local copies, waits for them, and re-layouts  19.1 us
    pallas_call x1, Pallas kernels, on_device(): pl.pallas_call(ffn_kernel, grid=(hidden_units // tile,), out_shape=shape(...  7.52 us

commit v1 on v0

v1 whole, which is shorter than its diff:
```python
import functools
import jax
import jax.numpy as jnp
from jax import lax
from jax.experimental import pallas as pl
from jax.experimental.pallas import tpu as pltpu
from jax.sharding import PartitionSpec as P

HEADS = 64
HEAD_DIM = 64
GROUPS = 2
NSTATE = 128
BLOCK = 128
ROW_EPS = 0.1
HEAD_EPS = 1.0
LANES = 128
F32 = jnp.float32
BF16 = jnp.bfloat16
ROWX = 4
GROUPED = 8
RIM = 16
PACK = 80
VMEM = pltpu.VMEM
MESH = pl.DeviceIdType.MESH


def vmem_specs(count):
    return [pl.BlockSpec(memory_space=VMEM)] * count


def cost(flops, moved):
    return pl.CostEstimate(flops=flops, bytes_accessed=moved, transcendentals=0)


def dot(a, b, dims, precision=None):
    return lax.dot_general(a, b, (dims, ((), ())), preferred_element_type=F32, precision=precision)


def eye(count):
    row = lax.broadcasted_iota(jnp.int32, (count, count), 0)
    col = lax.broadcasted_iota(jnp.int32, (count, count), 1)
    return jnp.where(row == col, 1.0, 0.0).astype(F32)


def upright(flat):
    return dot(flat, eye(flat.shape[0]), ((0,), (0,)), lax.Precision.HIGHEST)


def silu(v):
    return v / (1.0 + jnp.exp(-v))


def conv_rows(signal, rim, weight):
    taps = weight.shape[1]
    joined = jnp.concatenate([rim.astype(F32), signal.astype(F32)], axis=1)
    running = weight[:, taps - 1 : taps] * joined[:, LANES:]
    for back in range(1, taps):
        moved = pltpu.roll(joined, back, 1)[:, LANES:]
        running = running + weight[:, taps - 1 - back : taps - back] * moved
    return silu(running)


def prefix_decays(dt_ref, rate_ref):
    dt = dt_ref[...]
    step = jnp.maximum(dt, 0.0) + jnp.log1p(jnp.exp(-jnp.abs(dt)))
    rate = jnp.where(eye(dt.shape[0]) > 0.0, rate_ref[...], 0.0)
    log_decay = -step * jnp.sum(rate, axis=1, keepdims=True)
    length = dt.shape[1]
    row = lax.broadcasted_iota(jnp.int32, (length, length), 0)
    col = lax.broadcasted_iota(jnp.int32, (length, length), 1)
    upper = jnp.where(row <= col, 1.0, 0.0).astype(F32)
    lower = jnp.where(row >= col, 1.0, 0.0).astype(F32)
    high = lax.Precision.HIGHEST
    cum = dot(log_decay, upper, ((1,), (0,)), high)
    cum_col = dot(lower, log_decay, ((1,), (1,)), high)
    return step, cum, cum_col


def remote(source, target, send, recv, **where):
    return pltpu.make_async_remote_copy(
        src_ref=source, dst_ref=target, send_sem=send, recv_sem=recv, device_id=where, device_id_type=MESH
    )


def offsets(ep_size):
    deep = ep_size // ROWX
    hops = [(dz, dx) for dz in range(deep) for dx in range(ROWX)]
    return sorted(hops, key=lambda h: min(h[0], deep - h[0]) + min(h[1], ROWX - h[1]))


def layer_kernel(
    rows_hbm, gain_hbm, routes_hbm, logit_hbm, x_hbm, tapx_hbm, b_hbm, tapb_hbm, c_hbm, tapc_hbm,
    dt_hbm, rate_hbm, z_hbm, hgain_hbm, gate_hbm, up_hbm, down_hbm,
    mixed_ref, moe_ref,
    rows_ref, gain_ref, routes_ref, logit_ref, x_ref, tapx_ref, b_ref, tapb_ref, c_ref, tapc_ref,
    dt_ref, rate_ref, z_ref, hgain_ref, gu_ref, down_ref,
    rank_ref, weight_ref, pick_ref, outbox, landed, shrink_ref, grow_ref, xall, part, sibp, rs_out, rs_in,
    ret_out, returned,
    rim_out, rim_in, xrim, brim, crim, tap_col, tapb_col, tapc_col, gain_col,
    step_ref, cum_ref, col_ref, score_ref, bconv_ref, cconv_ref, xs_ref, y_ref,
    pre1_out, pre1_in, pre2_out, pre2_in, pre3_out, pre3_in, ex_ref, exr_ref,
    in_sem, box_send, box_recv, rim_send, rim_recv, ag_send, ag_recv, sib_send, sib_recv,
    dd_send, dd_recv, rs_send, rs_recv, ret_send, ret_recv, p1_send, p1_recv, p2_send, p2_recv, p3_send, p3_recv,
    *, ep_size, tp_size,
):
    me, lane = lax.axis_index("ep"), lax.axis_index("tp")
    deep, chips = ep_size // ROWX, tp_size // 2
    far = chips // 2
    z, x = me // ROWX, me % ROWX
    chip, core = lane // 2, lane % 2
    tokens, features = rows_ref.shape
    width = features // tp_size
    heads, length = dt_ref.shape
    pad = outbox.shape[1]
    capacity = xall.shape[1] // ep_size
    hops = offsets(ep_size)
    teams = ep_size // GROUPED
    span = GROUPED * capacity
    half = span // 2
    wide = GROUPED * pad

    loads = {}

    def load(name, source, target):
        copy = pltpu.make_async_copy(source, target, in_sem.at[len(loads)])
        copy.start()
        loads[name] = copy

    load("rows", rows_hbm, rows_ref)
    load("routes", routes_hbm, routes_ref)
    load("logit", logit_hbm, logit_ref)
    load("gain", gain_hbm, gain_ref)
    load("x", x_hbm, x_ref)
    load("b", b_hbm, b_ref)
    load("c", c_hbm, c_ref)
    load("tapx", tapx_hbm, tapx_ref)
    load("tapb", tapb_hbm, tapb_ref)
    load("tapc", tapc_hbm, tapc_ref)
    load("dt", dt_hbm, dt_ref)
    load("rate", rate_hbm, rate_ref)
    hidden_units = down_ref.shape[0]
    main = hidden_units // 256 * 256
    rest = hidden_units - main
    load("gate", gate_hbm.at[0, pl.ds(0, main), :], gu_ref.at[pl.ds(0, main), :])
    load("up", up_hbm.at[0, pl.ds(0, main), :], gu_ref.at[pl.ds(main, main), :])
    load("gate2", gate_hbm.at[0, pl.ds(main, rest), :], gu_ref.at[pl.ds(2 * main, rest), :])
    load("up2", up_hbm.at[0, pl.ds(main, rest), :], gu_ref.at[pl.ds(2 * main + rest, rest), :])
    load("down", down_hbm.at[0], down_ref)
    load("z", z_hbm, z_ref)
    load("hgain", hgain_hbm, hgain_ref)

    barrier = pltpu.get_barrier_semaphore()
    for hop in range(1, ep_size):
        pl.semaphore_signal(barrier, 1, device_id={"ep": (me + hop) % ep_size}, device_id_type=MESH)
    around = [((chip + 1) % chips) * 2 + core, ((chip + chips - 1) % chips) * 2 + core]
    sibling = chip * 2 + 1 - core
    for other in around + [sibling]:
        pl.semaphore_signal(barrier, 1, device_id={"tp": other}, device_id_type=MESH)

    for name in ("routes", "logit"):
        loads[name].wait()
    routes = routes_ref[...]
    logit = logit_ref[...]
    first = 1.0 / (1.0 + jnp.exp(logit[1:2] - logit[0:1]))
    second = 1.0 / (1.0 + jnp.exp(logit[0:1] - logit[1:2]))
    number = lax.broadcasted_iota(jnp.int32, (ep_size, tokens), 0)
    in_first = number == routes[0:1]
    in_second = number == routes[1:2]
    hits = jnp.where(in_first, 1.0, 0.0) + jnp.where(in_second, 1.0, 0.0)
    row = lax.broadcasted_iota(jnp.int32, (tokens, tokens), 0)
    col = lax.broadcasted_iota(jnp.int32, (tokens, tokens), 1)
    earlier = jnp.where(row < col, 1.0, 0.0).astype(BF16)
    rank = dot(hits.astype(BF16), earlier, ((1,), (0,)))
    weight_ref[...] = jnp.where(in_first, first, 0.0) + jnp.where(in_second, second, 0.0)
    rank_ref[...] = jnp.where(hits > 0.0, rank, -1.0)
    srow = lax.broadcasted_iota(jnp.int32, (span, wide), 0)
    scol = lax.broadcasted_iota(jnp.int32, (span, wide), 1)
    grow = lax.broadcasted_iota(jnp.int32, (wide, span), 0)
    gcol = lax.broadcasted_iota(jnp.int32, (wide, span), 1)
    shrink = jnp.zeros((span, wide), F32)
    grown = jnp.zeros((wide, span), F32)
    for slot in range(GROUPED):
        low, gap = slot * pad, slot * (pad - capacity)
        shrink = jnp.where((scol - srow == gap) & (scol >= low) & (scol < low + capacity), 1.0, shrink)
        grown = jnp.where((grow - gcol == gap) & (grow >= low) & (grow < low + capacity), 1.0, grown)
    shrink_ref[...] = shrink.astype(BF16)
    grow_ref[...] = grown.astype(BF16)
    for name in ("rows", "gain"):
        loads[name].wait()
    values = rows_ref[...].astype(F32)
    scale = lax.rsqrt(jnp.mean(values * values, axis=1, keepdims=True) + ROW_EPS)
    mine = pl.ds(pl.multiple_of(lane * width, LANES), width)
    normed = (rows_ref[:, mine].astype(F32) * scale * gain_ref[:, mine]).astype(BF16)
    place = lax.broadcasted_iota(jnp.int32, (pad, tokens), 0).astype(F32)

    def ahead(j):
        dz, dx = hops[j]
        return ((z + dz) % deep) * ROWX + (x + dx) % ROWX

    def behind(j):
        dz, dx = hops[j]
        return ((z + deep - dz) % deep) * ROWX + (x + ROWX - dx) % ROWX

    def box(j):
        return remote(outbox.at[j], landed.at[j], box_send.at[j], box_recv.at[j], ep=ahead(j))

    def back(j):
        return remote(ret_out.at[j], returned.at[j], ret_send.at[j], ret_recv.at[j], ep=behind(j))

    def dispatch(team):
        ones = []
        picks = []
        for slot in range(GROUPED):
            expert = ahead(team * GROUPED + slot)
            same = place == rank_ref[pl.ds(expert, 1), :]
            ones.append(jnp.where(same, 1.0, 0.0))
            picks.append(jnp.where(same, weight_ref[pl.ds(expert, 1), :], 0.0))
        pick_ref[team * wide : (team + 1) * wide, :] = jnp.concatenate(picks, axis=0).astype(BF16)
        chosen = dot(jnp.concatenate(ones, axis=0).astype(BF16), normed, ((1,), (0,)))
        for slot in range(GROUPED):
            j = team * GROUPED + slot
            piece = chosen[slot * pad : (slot + 1) * pad].astype(BF16)
            if j:
                outbox[j] = piece
                box(j).start()
            else:
                landed[j] = piece

    def packed(ref, team):
        pieces = [ref[team * GROUPED + slot].astype(F32) for slot in range(GROUPED)]
        return jnp.concatenate(pieces, axis=0).astype(BF16)

    group = pl.ds(pl.multiple_of(lane * heads // (HEADS // GROUPS) * NSTATE, NSTATE), NSTATE)
    value_rows = x_ref.shape[0]
    pickrow = lax.broadcasted_iota(jnp.int32, (RIM, LANES), 0)
    picklane = lax.broadcasted_iota(jnp.int32, (RIM, LANES), 1)
    edge = jnp.where(picklane == pickrow + (LANES - RIM), 1.0, 0.0).astype(BF16)
    end = slice(length - LANES, length)
    rim = remote(rim_out, rim_in, rim_send.at[0], rim_recv.at[0], ep=(me + 1) % ep_size)

    def send_rims():
        for name in ("x", "b", "c"):
            loads[name].wait()

        @pl.when(me + 1 < ep_size)
        def _():
            rim_out[:, :value_rows] = dot(edge, x_ref[:, end], ((1,), (1,))).astype(BF16)
            rim_out[:, value_rows : value_rows + NSTATE] = dot(edge, b_ref[group, end], ((1,), (1,))).astype(BF16)
            rim_out[:, value_rows + NSTATE :] = dot(edge, c_ref[group, end], ((1,), (1,))).astype(BF16)
            rim.start()

    def columns():
        for name in ("tapx", "tapb", "tapc", "dt", "rate", "hgain"):
            loads[name].wait()
        tap_col[...] = upright(tapx_ref[...])
        tapb_col[...] = upright(tapb_ref[...])
        tapc_col[...] = upright(tapc_ref[...])
        top = lax.broadcasted_iota(jnp.int32, (8, LANES), 0) == 0
        flat = jnp.broadcast_to(hgain_ref[...], (8, hgain_ref.shape[1]))
        gain_col[...] = dot(flat, jnp.where(top, 1.0, 0.0), ((0,), (0,)), lax.Precision.HIGHEST)
        step, cum, cum_col = prefix_decays(dt_ref, rate_ref)
        step_ref[...] = step
        cum_ref[...] = cum
        for head in range(heads):
            col_ref[head] = jnp.broadcast_to(cum_col[:, head : head + 1], (length, LANES))

    def open_rims():
        @pl.when(me > 0)
        def _():
            rim.wait_recv()
            xrim[...] = dot(rim_in[:, :value_rows], edge, ((0,), (0,)))
            brim[...] = dot(rim_in[:, value_rows : value_rows + NSTATE], edge, ((0,), (0,)))
            crim[...] = dot(rim_in[:, value_rows + NSTATE :], edge, ((0,), (0,)))

        @pl.when(me == 0)
        def _():
            for ref in (xrim, brim, crim):
                ref[...] = jnp.zeros_like(ref)

    def state_streams():
        b_conv = conv_rows(b_ref[group, :], brim[...], tapb_col[group, :]).astype(BF16)
        c_conv = conv_rows(c_ref[group, :], crim[...], tapc_col[group, :]).astype(BF16)
        bconv_ref[...] = b_conv
        cconv_ref[...] = c_conv
        score_ref[...] = dot(b_conv, c_conv, ((0,), (0,)))

    def split(reach):
        high = reach.astype(BF16).astype(F32)
        at = lax.broadcasted_iota(jnp.int32, (RIM, NSTATE), 0)
        wideness = (RIM, NSTATE)
        low = jnp.broadcast_to(reach - high, wideness)
        return jnp.where(at == 0, jnp.broadcast_to(high, wideness), jnp.where(at == 1, low, 0.0)).astype(BF16)

    def joinup(block):
        block = block.astype(F32)
        return block[0:1] + block[1:2]

    def end_state(head):
        rows = slice(head * HEAD_DIM, (head + 1) * HEAD_DIM)
        value = conv_rows(x_ref[rows, :], xrim[rows, :], tap_col[rows, :])
        own = cum_ref[head : head + 1, :]
        last = own[:, length - 1 :]
        xs = value * step_ref[head : head + 1, :]
        tail = xs * jnp.exp(last - own)
        pre1_out[head, :HEAD_DIM] = dot(tail.astype(BF16), bconv_ref[...], ((1,), (1,))).astype(BF16)
        pre1_out[head, HEAD_DIM:] = split(jnp.broadcast_to(jnp.exp(last), (1, NSTATE)))
        xs_ref[rows, :] = xs.astype(BF16)

    def local_y(head):
        rows = slice(head * HEAD_DIM, (head + 1) * HEAD_DIM)
        own = cum_ref[head : head + 1, :]
        brow = lax.broadcasted_iota(jnp.int32, (BLOCK, BLOCK), 0)
        bcol = lax.broadcasted_iota(jnp.int32, (BLOCK, BLOCK), 1)
        causal = brow <= bcol
        for target in range(length // BLOCK):
            at = slice(target * BLOCK, (target + 1) * BLOCK)
            pieces = []
            for source in range(target + 1):
                of = slice(source * BLOCK, (source + 1) * BLOCK)
                gap = own[:, at] - col_ref[head, of, :]
                if source == target:
                    gap = jnp.where(causal, gap, -jnp.inf)
                pieces.append((score_ref[of, at] * jnp.exp(gap)).astype(BF16))
            mask = pieces[0] if target == 0 else jnp.concatenate(pieces, axis=0)
            y_ref[rows, at] = dot(xs_ref[rows, : (target + 1) * BLOCK], mask, ((1,), (0,)))

    def close(head):
        rows = slice(head * HEAD_DIM, (head + 1) * HEAD_DIM)
        carried = dot(pre3_in[head], cconv_ref[...], ((1,), (0,)))
        y = y_ref[rows, :] + carried * jnp.exp(cum_ref[head : head + 1, :])
        gated = y * silu(z_ref[rows, :].astype(F32))
        norm = lax.rsqrt(jnp.mean(gated * gated, axis=0, keepdims=True) + HEAD_EPS)
        mixed_ref[rows, :] = (gated * norm * gain_col[rows, 0:1]).astype(BF16)

    def pre1(dx):
        head = (x + dx) % ROWX
        return remote(pre1_out.at[head], pre1_in.at[x], p1_send.at[dx], p1_recv.at[dx], ep=z * ROWX + head)

    def pre2(dz):
        return remote(pre2_out, pre2_in.at[z], p2_send.at[dz], p2_recv.at[dz], ep=((z + dz) % deep) * ROWX + x)

    def pre3(dx):
        spot = (x + dx) % ROWX
        return remote(pre3_out.at[spot], pre3_in.at[x], p3_send.at[dx], p3_recv.at[dx], ep=z * ROWX + spot)

    def spread_states():
        for dx in range(1, ROWX):
            pre1(dx).start()
        pre1_in[x] = pre1_out[x]

    def row_totals():
        for dx in range(1, ROWX):
            pre1(dx).wait_recv()
        total = jnp.zeros((HEAD_DIM, NSTATE), F32)
        reach = jnp.ones((1, NSTATE), F32)
        for spot in range(ROWX):
            ex_ref[spot] = total
            exr_ref[spot] = jnp.broadcast_to(reach, exr_ref.shape[1:])
            hold = joinup(pre1_in[spot, HEAD_DIM:])
            total = pre1_in[spot, :HEAD_DIM].astype(F32) + hold * total
            reach = reach * hold
        pre2_out[:HEAD_DIM] = total.astype(BF16)
        pre2_out[HEAD_DIM:] = split(reach)
        for dz in range(1, deep):

            @pl.when(z + dz < deep)
            def _(dz=dz):
                pre2(dz).start()

    def incoming():
        for dz in range(1, deep):

            @pl.when(z >= dz)
            def _(dz=dz):
                pre2(dz).wait_recv()

        prior = jnp.zeros((HEAD_DIM, NSTATE), F32)
        for level in range(deep - 1):
            after = pre2_in[level, :HEAD_DIM].astype(F32) + joinup(pre2_in[level, HEAD_DIM:]) * prior
            prior = jnp.where(level < z, after, prior)
        for spot in range(ROWX):
            pre3_out[spot] = (ex_ref[spot] + exr_ref[spot, 0:1] * prior).astype(BF16)
        for dx in range(1, ROWX):
            pre3(dx).start()
        pre3_in[x] = pre3_out[x]

    def at_rows(team, d, step):
        if step < far - 1:
            return team * span, span
        return team * span + d * half, half

    def ag(d, team, step):
        sign = 1 - 2 * d
        origin = ((chip + chips - sign * step) % chips) * 2 + core
        start, count = at_rows(team, d, step)
        ref = xall.at[origin, pl.ds(start, count), :]
        return remote(ref, ref, ag_send.at[d, team, step], ag_recv.at[d, team, step], tp=around[d])

    def sib(team, d, step):
        sign = 1 - 2 * d
        origin = ((chip + chips - sign * (step + 1)) % chips) * 2 + core
        start, count = at_rows(team, d, step)
        ref = xall.at[origin, pl.ds(start, count), :]
        index = 0 if step < 0 else 1 + d * far + step
        return remote(ref, ref, sib_send.at[team, index], sib_recv.at[team, index], tp=sibling)

    def arrivals():
        return [(0, -1)] + [(d, step) for step in range(far) for d in range(2)]

    def gather_own(team):
        for slot in range(GROUPED):
            if team or slot:
                box(team * GROUPED + slot).wait_recv()
        block = dot(shrink_ref[...], packed(landed, team), ((1,), (0,))).astype(BF16)
        xall[lane, team * span : (team + 1) * span, :] = block
        for d in range(2):
            ag(d, team, 0).start()
        sib(team, 0, -1).start()

    def gather_step(team, step):
        for d in range(2):
            ag(d, team, step).wait_recv()
            if step + 1 < far:
                ag(d, team, step + 1).start()
            sib(team, d, step).start()

    def ffn(team):
        for d, step in arrivals():
            sib(team, d, step).wait_recv()
        rows = slice(team * span, (team + 1) * span)
        tokens_in = jnp.concatenate([xall[i, rows, :] for i in range(tp_size)], axis=1)
        both = dot(tokens_in, gu_ref[...], ((1,), (1,)))
        hidden = (silu(both[:, :main]) * both[:, main : 2 * main]).astype(BF16)
        last = both[:, 2 * main :]
        extra = (silu(last) * pltpu.roll(last, rest, 1)).astype(BF16)[:, :rest]
        out = dot(hidden, down_ref[:main, :], ((1,), (0,))) + dot(extra, down_ref[main:, :], ((1,), (0,)))
        for i in range(tp_size):
            part[team, i % 2, i // 2] = out[:, i * width : (i + 1) * width].astype(BF16)
        for reach in order_of_need:
            cross(team, reach).start()

    order_of_need = [far]
    for away in range(far - 1, 0, -1):
        order_of_need += [away, chips - away]
    order_of_need.append(0)

    def cross(team, reach):
        at = (chip + reach) % chips
        return remote(
            part.at[team, 1 - core, at], sibp.at[team, at], dd_send.at[team, reach], dd_recv.at[team, reach], tp=sibling
        )

    def own_sum(team, reach):
        at = (chip + reach) % chips
        return part[team, core, at].astype(F32) + sibp[team, at].astype(F32)

    def rs(d, team, step):
        start, count = (d * half, half) if step == 0 else (0, span)
        return remote(
            rs_out.at[d, team, step, pl.ds(start, count), :], rs_in.at[d, team, step, pl.ds(start, count), :],
            rs_send.at[d, team, step], rs_recv.at[d, team, step], tp=around[d],
        )

    def scatter_first(team):
        cross(team, far).wait_recv()
        total = own_sum(team, far).astype(BF16)
        for d in range(2):
            cut = slice(d * half, (d + 1) * half)
            rs_out[d, team, 0, cut, :] = total[cut]
            rs(d, team, 0).start()

    def scatter_step(team, step):
        for d in range(2):
            reach = far - step if d == 0 else chips - (far - step)
            cross(team, reach).wait_recv()
            total = own_sum(team, reach)
            rs(d, team, step - 1).wait_recv()
            if step == 1:
                cut = slice(d * half, (d + 1) * half)
                other = slice((1 - d) * half, (2 - d) * half)
                rs_out[d, team, step, other, :] = total[other].astype(BF16)
                rs_out[d, team, step, cut, :] = (total[cut] + rs_in[d, team, 0, cut, :].astype(F32)).astype(BF16)
            else:
                rs_out[d, team, step] = (total + rs_in[d, team, step - 1].astype(F32)).astype(BF16)
            rs(d, team, step).start()

    def scatter_last(team):
        cross(team, 0).wait_recv()
        total = own_sum(team, 0)
        for d in range(2):
            rs(d, team, far - 1).wait_recv()
            total = total + rs_in[d, team, far - 1].astype(F32)
        spread = dot(grow_ref[...], total.astype(BF16), ((1,), (0,)))
        for slot in range(GROUPED):
            j = team * GROUPED + slot
            piece = spread[slot * pad : (slot + 1) * pad].astype(BF16)
            if j:
                ret_out[j] = piece
                back(j).start()
            else:
                returned[j] = piece

    pl.semaphore_wait(barrier, ep_size - 1 + len(around) + 1)
    for team in range(teams):
        dispatch(team)
    send_rims()
    columns()
    for team in range(teams):
        gather_own(team)
    open_rims()
    state_streams()
    for head in range(heads):
        end_state(head)
    spread_states()
    for step in range(far):
        for team in range(teams):
            gather_step(team, step)
        if step == 0:
            row_totals()
            local_y(0)
        elif step == 1:
            incoming()
            local_y(1)
        elif step == 2:
            local_y(2)
            local_y(3)
            for name in ("gate", "up", "gate2", "up2", "down", "z"):
                loads[name].wait()
    for team in range(teams):
        ffn(team)
        if team:
            scatter_first(team - 1)
    scatter_first(teams - 1)
    for step in range(1, far):
        for team in range(teams):
            scatter_step(team, step)
        if step == 1:
            for dx in range(1, ROWX):
                pre3(dx).wait_recv()
            close(0)
        elif step == 2:
            close(1)
            close(2)
        else:
            close(3)
    for team in range(teams):
        scatter_last(team)
    total = jnp.zeros((tokens, width), F32)
    for team in range(teams):
        for slot in range(GROUPED):
            if team or slot:
                back(team * GROUPED + slot).wait_recv()
        total = total + dot(pick_ref[team * wide : (team + 1) * wide, :], packed(returned, team), ((0,), (0,)))
    moe_ref[...] = total.astype(BF16)

    for j in range(1, ep_size):
        box(j).wait_send()
        back(j).wait_send()

    @pl.when(me + 1 < ep_size)
    def _():
        rim.wait_send()

    for dx in range(1, ROWX):
        pre1(dx).wait_send()
        pre3(dx).wait_send()
    for dz in range(1, deep):

        @pl.when(z + dz < deep)
        def _(dz=dz):
            pre2(dz).wait_send()

    for team in range(teams):
        for d in range(2):
            for step in range(far):
                ag(d, team, step).wait_send()
                rs(d, team, step).wait_send()
        for d, step in arrivals():
            sib(team, d, step).wait_send()
        for reach in range(chips):
            cross(team, reach).wait_send()


def on_device(
    x_in, z_in, dt_raw, decay_rate, b_in, c_in, conv_x, conv_b, conv_c, head_gain,
    moe_rows, moe_gain, routes, route_logit, w_gate, w_up, w_down,
):
    heads, length = dt_raw.shape
    value_rows = x_in.shape[0]
    taps = conv_x.shape[1]
    tp_size = lax.axis_size("tp")
    ep_size = lax.axis_size("ep")
    tokens, features = moe_rows.shape
    top = routes.shape[1]
    capacity = 2 * tokens * top // ep_size
    pad = (capacity + 7) // 8 * 8
    width = features // tp_size
    hidden_units = w_gate.shape[2]
    slots = ep_size * capacity
    deep, chips = ep_size // ROWX, tp_size // 2
    far, teams, span = chips // 2, ep_size // GROUPED, GROUPED * capacity
    dma = pltpu.SemaphoreType.DMA
    shape = jax.ShapeDtypeStruct
    groups = b_in.shape[0]

    mixed, moe = pl.pallas_call(
        functools.partial(layer_kernel, ep_size=ep_size, tp_size=tp_size),
        out_shape=(shape((value_rows, length), BF16), shape((tokens, width), BF16)),
        in_specs=[pl.BlockSpec(memory_space=pltpu.HBM)] * 17,
        out_specs=tuple(vmem_specs(2)),
        scratch_shapes=[
            VMEM((tokens, features), BF16), VMEM((1, features), F32), VMEM((top, tokens), jnp.int32), VMEM((top, tokens), F32),
            VMEM((value_rows, length), BF16), VMEM((taps, value_rows), F32),
            VMEM((groups, length), BF16), VMEM((taps, groups), F32), VMEM((groups, length), BF16), VMEM((taps, groups), F32),
            VMEM((heads, length), F32), VMEM((1, heads), F32), VMEM((value_rows, length), BF16), VMEM((1, value_rows), F32),
            VMEM((2 * hidden_units, features), BF16), VMEM((hidden_units, features), BF16),
            VMEM((ep_size, tokens), F32), VMEM((ep_size, tokens), F32), VMEM((ep_size * pad, tokens), BF16),
            VMEM((ep_size, pad, width), BF16), VMEM((ep_size, pad, width), BF16),
            VMEM((span, GROUPED * pad), BF16), VMEM((GROUPED * pad, span), BF16),
            VMEM((tp_size, slots, width), BF16),
            VMEM((teams, 2, chips, span, width), BF16), VMEM((teams, chips, span, width), BF16),
            VMEM((2, teams, far, span, width), BF16), VMEM((2, teams, far, span, width), BF16),
            VMEM((ep_size, pad, width), BF16), VMEM((ep_size, pad, width), BF16),
            VMEM((RIM, value_rows + 2 * NSTATE), BF16), VMEM((RIM, value_rows + 2 * NSTATE), BF16),
            VMEM((value_rows, LANES), F32), VMEM((NSTATE, LANES), F32), VMEM((NSTATE, LANES), F32),
            VMEM((value_rows, taps), F32), VMEM((groups, taps), F32), VMEM((groups, taps), F32),
            VMEM((value_rows, LANES), F32),
            VMEM((heads, length), F32), VMEM((heads, length), F32), VMEM((heads, length, LANES), F32),
            VMEM((length, length), F32), VMEM((NSTATE, length), BF16), VMEM((NSTATE, length), BF16),
            VMEM((value_rows, length), BF16), VMEM((value_rows, length), F32),
            VMEM((heads, PACK, NSTATE), BF16), VMEM((ROWX, PACK, NSTATE), BF16),
            VMEM((PACK, NSTATE), BF16), VMEM((deep, PACK, NSTATE), BF16),
            VMEM((ROWX, HEAD_DIM, NSTATE), BF16), VMEM((ROWX, HEAD_DIM, NSTATE), BF16),
            VMEM((ROWX, HEAD_DIM, NSTATE), F32), VMEM((ROWX, 8, NSTATE), F32),
            dma((19,)), dma((ep_size,)), dma((ep_size,)), dma((1,)), dma((1,)),
            dma((2, teams, far)), dma((2, teams, far)), dma((teams, 1 + 2 * far)), dma((teams, 1 + 2 * far)),
            dma((teams, chips)), dma((teams, chips)), dma((2, teams, far)), dma((2, teams, far)),
            dma((ep_size,)), dma((ep_size,)), dma((ROWX,)), dma((ROWX,)), dma((deep,)), dma((deep,)), dma((ROWX,)), dma((ROWX,)),
        ],
        compiler_params=pltpu.CompilerParams(collective_id=0, has_side_effects=True, vmem_limit_bytes=56 * 2**20),
        name="layer",
    )(
        moe_rows, moe_gain.reshape(1, features), routes.T, route_logit.T,
        x_in, conv_x.T, b_in, conv_b.T, c_in, conv_c.T, dt_raw, decay_rate.reshape(1, heads),
        z_in, head_gain.reshape(1, value_rows),
        jnp.swapaxes(w_gate, 1, 2), jnp.swapaxes(w_up, 1, 2), w_down,
    )
    return (mixed, moe.T)


def solution(mesh):
    return jax.shard_map(
        on_device,
        mesh=mesh,
        in_specs=(
            P("tp", "ep"), P("tp", "ep"), P("tp", "ep"), P("tp"), P(None, "ep"), P(None, "ep"),
            P("tp", None), P(), P(), P("tp"), P("ep", None), P(), P("ep", None), P("ep", None),
            P("ep", None, "tp"), P("ep", None, "tp"), P("ep", "tp", None),
        ),
        out_specs=(P("tp", "ep"), P("tp", "ep")),
        check_vma=False,
    )
```

time: 177 us -> 77 us (0.44)
  Pallas kernels: 148 us -> 73.1 us
  local copies, waits for them, and re-layouts: 27.3 us -> 3.02 us
    pallas_call x5 -> x1, Pallas kernels: 148 us -> 73.1 us  [on_device(): pl.pallas_call(functools.partial(layer_kernel, ep_size=ep_size, tp_size=t...]
    unnamed x42 -> x2, local copies, waits for them, and re-layouts: 19.1 us -> 3.02 us
    reshape x4 -> x0, local copies, waits for them, and re-layouts: 8.19 us -> none  [the longest x1 3.52 us: on_device(): partial.reshape(experts, capacity, features)]
where the time goes in v1:
time: 77 us; the launch traced here: 76.8 us
  Pallas kernels  73.1 us (95%)
  local copies, waits for them, and re-layouts  3.02 us (4%)
    pallas_call x1, Pallas kernels, on_device(): pl.pallas_call(functools.partial(layer_kernel, ep_size=ep_size, tp_size=t...  73.1 us
    unnamed x2, local copies, waits for them, and re-layouts  3.02 us

profile of v1, /device:TPU:8, one launch (start us, length us, event | category | flops | bytes accessed | tf_op | source)
XLA Modules:
  0.0 76.8 jit_solution(18049591914089793251)
XLA Ops:
  0.6 73.1 %layer.1 = (bf16[256,384]{1,0:T(8,128)(2,1)}, bf16[160,128]{1,0:T(8,128)(2,1)}) custom-call(bf16[160,2048]{1,0:T(8,128)(2,1)} %rows_hbm.1, f32[1,2048]{1,0:T(1,128)} %bitcast.14, s32[2,160]{1,0:T(2,128)} %bitcast.18, f32[2,160]{1,0:T(2,128)} %bitcast.19, bf16[256,384]{1,0:T(8,128)(2,1)} %x_hbm.1, f32[4,256]{1,0:T(4,128)} %bitcast.15, ...), custom_call_target="tpu_custom_call" | custom-call | tf_op jit(solution)/shard_map/layer/pallas_call | solution.py:606
  73.8 1.6 %copy.21 = bf16[256,384]{1,0:T(8,128)(2,1)} copy(bf16[256,384]{1,0:T(8,128)(2,1)} %get-tuple-element.8) | data formatting | bytes 393216
  75.4 1.4 %copy.22 = bf16[128,160]{0,1:T(8,128)(2,1)} copy(bf16[128,160]{0,1:T(8,128)(2,1)} %bitcast.13) | data formatting | bytes 81920

commit v2 on v1

--- a/solution.py
+++ b/solution.py
@@ -20,6 +20,21 @@
 GROUPED = 8
 RIM = 16
 PACK = 80
+PLAN = (
+    ("columns",), ("decays",), ("turn", 0), ("turn", 1), ("turn", 2), ("turn", 3), ("gather_own", 0), ("open_rims",),
+    ("b_stream",), ("c_stream",), ("gather_own", 1), ("end_state", 0), ("end_state", 1), ("end_state", 2),
+    ("end_state", 3), ("gather_step", 0, 0), ("scores",), ("spread_states",), ("local_y", 0), ("local_y", 1),
+    ("local_y", 2), ("gather_own", 2), ("local_y", 3), ("gather_step", 1, 0), ("gather_own", 3),
+    ("gather_step", 0, 1), ("gather_step", 2, 0), ("gather_step", 1, 1), ("gather_step", 3, 0), ("gather_step", 0, 2),
+    ("gather_step", 2, 1), ("row_totals",), ("gather_step", 1, 2), ("gather_step", 3, 1), ("gather_step", 0, 3),
+    ("gather_step", 2, 2), ("ffn", 0), ("gather_step", 1, 3), ("gather_step", 3, 2), ("gather_step", 2, 3),
+    ("ffn", 1), ("gather_step", 3, 3), ("scatter_first", 0), ("ffn", 2), ("ffn", 3), ("scatter_first", 1),
+    ("scatter_step", 0, 1), ("incoming",), ("scatter_first", 2), ("scatter_first", 3), ("scatter_step", 1, 1),
+    ("scatter_step", 0, 2), ("scatter_step", 2, 1), ("scatter_step", 3, 1), ("scatter_step", 1, 2),
+    ("scatter_step", 0, 3), ("close", 0), ("close", 1), ("close", 2), ("scatter_step", 2, 2), ("close", 3),
+    ("scatter_step", 3, 2), ("scatter_step", 1, 3), ("scatter_last", 0), ("scatter_step", 2, 3),
+    ("scatter_step", 3, 3), ("scatter_last", 1), ("scatter_last", 2), ("scatter_last", 3),
+)
 VMEM = pltpu.VMEM
 MESH = pl.DeviceIdType.MESH
 
@@ -85,7 +100,9 @@
 def offsets(ep_size):
     deep = ep_size // ROWX
     hops = [(dz, dx) for dz in range(deep) for dx in range(ROWX)]
-    return sorted(hops, key=lambda h: min(h[0], deep - h[0]) + min(h[1], ROWX - h[1]))
+    near = sorted(hops, key=lambda h: min(h[0], deep - h[0]) + min(h[1], ROWX - h[1]))
+    first, second = near[:GROUPED], near[GROUPED : 2 * GROUPED]
+    return first + near[2 * GROUPED :] + second
 
 
 def layer_kernel(
@@ -93,8 +110,8 @@
     dt_hbm, rate_hbm, z_hbm, hgain_hbm, gate_hbm, up_hbm, down_hbm,
     mixed_ref, moe_ref,
     rows_ref, gain_ref, routes_ref, logit_ref, x_ref, tapx_ref, b_ref, tapb_ref, c_ref, tapc_ref,
-    dt_ref, rate_ref, z_ref, hgain_ref, gu_ref, down_ref,
-    rank_ref, weight_ref, pick_ref, outbox, landed, shrink_ref, grow_ref, xall, part, sibp, rs_out, rs_in,
+    dt_ref, rate_ref, z_ref, hgain_ref, gu_ref, gut_ref, down_ref,
+    rank_ref, weight_ref, pick_ref, outbox, landed, xall, part, sibp, rs_out, rs_in,
     ret_out, returned,
     rim_out, rim_in, xrim, brim, crim, tap_col, tapb_col, tapc_col, gain_col,
     step_ref, cum_ref, col_ref, score_ref, bconv_ref, cconv_ref, xs_ref, y_ref,
@@ -173,18 +190,6 @@
     rank = dot(hits.astype(BF16), earlier, ((1,), (0,)))
     weight_ref[...] = jnp.where(in_first, first, 0.0) + jnp.where(in_second, second, 0.0)
     rank_ref[...] = jnp.where(hits > 0.0, rank, -1.0)
-    srow = lax.broadcasted_iota(jnp.int32, (span, wide), 0)
-    scol = lax.broadcasted_iota(jnp.int32, (span, wide), 1)
-    grow = lax.broadcasted_iota(jnp.int32, (wide, span), 0)
-    gcol = lax.broadcasted_iota(jnp.int32, (wide, span), 1)
-    shrink = jnp.zeros((span, wide), F32)
-    grown = jnp.zeros((wide, span), F32)
-    for slot in range(GROUPED):
-        low, gap = slot * pad, slot * (pad - capacity)
-        shrink = jnp.where((scol - srow == gap) & (scol >= low) & (scol < low + capacity), 1.0, shrink)
-        grown = jnp.where((grow - gcol == gap) & (grow >= low) & (grow < low + capacity), 1.0, grown)
-    shrink_ref[...] = shrink.astype(BF16)
-    grow_ref[...] = grown.astype(BF16)
     for name in ("rows", "gain"):
         loads[name].wait()
     values = rows_ref[...].astype(F32)
@@ -258,6 +263,8 @@
         top = lax.broadcasted_iota(jnp.int32, (8, LANES), 0) == 0
         flat = jnp.broadcast_to(hgain_ref[...], (8, hgain_ref.shape[1]))
         gain_col[...] = dot(flat, jnp.where(top, 1.0, 0.0), ((0,), (0,)), lax.Precision.HIGHEST)
+
+    def decays():
         step, cum, cum_col = prefix_decays(dt_ref, rate_ref)
         step_ref[...] = step
         cum_ref[...] = cum
@@ -277,12 +284,22 @@
             for ref in (xrim, brim, crim):
                 ref[...] = jnp.zeros_like(ref)
 
-    def state_streams():
-        b_conv = conv_rows(b_ref[group, :], brim[...], tapb_col[group, :]).astype(BF16)
-        c_conv = conv_rows(c_ref[group, :], crim[...], tapc_col[group, :]).astype(BF16)
-        bconv_ref[...] = b_conv
-        cconv_ref[...] = c_conv
-        score_ref[...] = dot(b_conv, c_conv, ((0,), (0,)))
+    def b_stream():
+        bconv_ref[...] = conv_rows(b_ref[group, :], brim[...], tapb_col[group, :]).astype(BF16)
+
+    def c_stream():
+        cconv_ref[...] = conv_rows(c_ref[group, :], crim[...], tapc_col[group, :]).astype(BF16)
+
+    def scores():
+        score_ref[...] = dot(bconv_ref[...], cconv_ref[...], ((0,), (0,)))
+
+    def turn(quarter):
+        if quarter == 0:
+            for name in ("gate", "up", "gate2", "up2", "down", "z"):
+                loads[name].wait()
+        cut = features // 4
+        at = slice(quarter * cut, (quarter + 1) * cut)
+        gut_ref[at, :] = gu_ref[:, at].T
 
     def split(reach):
         high = reach.astype(BF16).astype(F32)
@@ -325,6 +342,9 @@
             y_ref[rows, at] = dot(xs_ref[rows, : (target + 1) * BLOCK], mask, ((1,), (0,)))
 
     def close(head):
+        if head == 0:
+            for dx in range(1, ROWX):
+                pre3(dx).wait_recv()
         rows = slice(head * HEAD_DIM, (head + 1) * HEAD_DIM)
         carried = dot(pre3_in[head], cconv_ref[...], ((1,), (0,)))
         y = y_ref[rows, :] + carried * jnp.exp(cum_ref[head : head + 1, :])
@@ -411,8 +431,7 @@
         for slot in range(GROUPED):
             if team or slot:
                 box(team * GROUPED + slot).wait_recv()
-        block = dot(shrink_ref[...], packed(landed, team), ((1,), (0,))).astype(BF16)
-        xall[lane, team * span : (team + 1) * span, :] = block
+        xall[lane, team * span : (team + 1) * span, :] = packed(landed, team)
         for d in range(2):
             ag(d, team, 0).start()
         sib(team, 0, -1).start()
@@ -429,11 +448,11 @@
             sib(team, d, step).wait_recv()
         rows = slice(team * span, (team + 1) * span)
         tokens_in = jnp.concatenate([xall[i, rows, :] for i in range(tp_size)], axis=1)
-        both = dot(tokens_in, gu_ref[...], ((1,), (1,)))
+        both = dot(tokens_in, gut_ref[...], ((1,), (0,)))
         hidden = (silu(both[:, :main]) * both[:, main : 2 * main]).astype(BF16)
         last = both[:, 2 * main :]
         extra = (silu(last) * pltpu.roll(last, rest, 1)).astype(BF16)[:, :rest]
-        out = dot(hidden, down_ref[:main, :], ((1,), (0,))) + dot(extra, down_ref[main:, :], ((1,), (0,)))
+        out = dot(jnp.concatenate([hidden, extra], axis=1), down_ref[...], ((1,), (0,)))
         for i in range(tp_size):
             part[team, i % 2, i // 2] = out[:, i * width : (i + 1) * width].astype(BF16)
         for reach in order_of_need:
@@ -490,10 +509,9 @@
         for d in range(2):
             rs(d, team, far - 1).wait_recv()
             total = total + rs_in[d, team, far - 1].astype(F32)
-        spread = dot(grow_ref[...], total.astype(BF16), ((1,), (0,)))
         for slot in range(GROUPED):
             j = team * GROUPED + slot
-            piece = spread[slot * pad : (slot + 1) * pad].astype(BF16)
+            piece = total[slot * pad : (slot + 1) * pad].astype(BF16)
             if j:
                 ret_out[j] = piece
                 back(j).start()
@@ -501,57 +519,26 @@
                 returned[j] = piece
 
     pl.semaphore_wait(barrier, ep_size - 1 + len(around) + 1)
-    for team in range(teams):
+    for team in (0, 2, 1, 3):
         dispatch(team)
     send_rims()
-    columns()
-    for team in range(teams):
-        gather_own(team)
-    open_rims()
-    state_streams()
-    for head in range(heads):
-        end_state(head)
-    spread_states()
-    for step in range(far):
+    parts = (
+        columns, decays, turn, gather_own, gather_step, ffn, scatter_first, scatter_step, scatter_last, open_rims,
+        b_stream, c_stream, scores, end_state, spread_states, local_y, row_totals, incoming, close,
+    )
+    named = {part.__name__: part for part in parts}
+    for step in PLAN:
+        named[step[0]](*step[1:])
+    def combine():
+        total = jnp.zeros((tokens, width), F32)
         for team in range(teams):
-            gather_step(team, step)
-        if step == 0:
-            row_totals()
-            local_y(0)
-        elif step == 1:
-            incoming()
-            local_y(1)
-        elif step == 2:
-            local_y(2)
-            local_y(3)
-            for name in ("gate", "up", "gate2", "up2", "down", "z"):
-                loads[name].wait()
-    for team in range(teams):
-        ffn(team)
-        if team:
-            scatter_first(team - 1)
-    scatter_first(teams - 1)
-    for step in range(1, far):
-        for team in range(teams):
-            scatter_step(team, step)
-        if step == 1:
-            for dx in range(1, ROWX):
-                pre3(dx).wait_recv()
-            close(0)
-        elif step == 2:
-            close(1)
-            close(2)
-        else:
-            close(3)
-    for team in range(teams):
-        scatter_last(team)
-    total = jnp.zeros((tokens, width), F32)
-    for team in range(teams):
-        for slot in range(GROUPED):
-            if team or slot:
-                back(team * GROUPED + slot).wait_recv()
-        total = total + dot(pick_ref[team * wide : (team + 1) * wide, :], packed(returned, team), ((0,), (0,)))
-    moe_ref[...] = total.astype(BF16)
+            for slot in range(GROUPED):
+                if team or slot:
+                    back(team * GROUPED + slot).wait_recv()
+            total = total + dot(pick_ref[team * wide : (team + 1) * wide, :], packed(returned, team), ((0,), (0,)))
+        moe_ref[...] = total.astype(BF16)
+
+    combine()
 
     for j in range(1, ep_size):
         box(j).wait_send()
@@ -579,6 +566,17 @@
             sib(team, d, step).wait_send()
         for reach in range(chips):
             cross(team, reach).wait_send()
+
+
+def emit_kernel(mixed_ref, moe_ref, mixed_out, moe_out, sems):
+    copies = [
+        pltpu.make_async_copy(mixed_ref, mixed_out, sems.at[0]),
+        pltpu.make_async_copy(moe_ref, moe_out, sems.at[1]),
+    ]
+    for copy in copies:
+        copy.start()
+    for copy in copies:
+        copy.wait()
 
 
 def on_device(
@@ -593,7 +591,7 @@
     tokens, features = moe_rows.shape
     top = routes.shape[1]
     capacity = 2 * tokens * top // ep_size
-    pad = (capacity + 7) // 8 * 8
+    pad = capacity
     width = features // tp_size
     hidden_units = w_gate.shape[2]
     slots = ep_size * capacity
@@ -605,7 +603,7 @@
 
     mixed, moe = pl.pallas_call(
         functools.partial(layer_kernel, ep_size=ep_size, tp_size=tp_size),
-        out_shape=(shape((value_rows, length), BF16), shape((tokens, width), BF16)),
+        out_shape=(VMEM((value_rows, length), BF16), VMEM((tokens, width), BF16)),
         in_specs=[pl.BlockSpec(memory_space=pltpu.HBM)] * 17,
         out_specs=tuple(vmem_specs(2)),
         scratch_shapes=[
@@ -613,10 +611,9 @@
             VMEM((value_rows, length), BF16), VMEM((taps, value_rows), F32),
             VMEM((groups, length), BF16), VMEM((taps, groups), F32), VMEM((groups, length), BF16), VMEM((taps, groups), F32),
             VMEM((heads, length), F32), VMEM((1, heads), F32), VMEM((value_rows, length), BF16), VMEM((1, value_rows), F32),
-            VMEM((2 * hidden_units, features), BF16), VMEM((hidden_units, features), BF16),
+            VMEM((2 * hidden_units, features), BF16), VMEM((features, 2 * hidden_units), BF16), VMEM((hidden_units, features), BF16),
             VMEM((ep_size, tokens), F32), VMEM((ep_size, tokens), F32), VMEM((ep_size * pad, tokens), BF16),
             VMEM((ep_size, pad, width), BF16), VMEM((ep_size, pad, width), BF16),
-            VMEM((span, GROUPED * pad), BF16), VMEM((GROUPED * pad, span), BF16),
             VMEM((tp_size, slots, width), BF16),
             VMEM((teams, 2, chips, span, width), BF16), VMEM((teams, chips, span, width), BF16),
             VMEM((2, teams, far, span, width), BF16), VMEM((2, teams, far, span, width), BF16),
@@ -637,7 +634,7 @@
             dma((teams, chips)), dma((teams, chips)), dma((2, teams, far)), dma((2, teams, far)),
             dma((ep_size,)), dma((ep_size,)), dma((ROWX,)), dma((ROWX,)), dma((deep,)), dma((deep,)), dma((ROWX,)), dma((ROWX,)),
         ],
-        compiler_params=pltpu.CompilerParams(collective_id=0, has_side_effects=True, vmem_limit_bytes=56 * 2**20),
+        compiler_params=pltpu.CompilerParams(collective_id=0, has_side_effects=True, vmem_limit_bytes=60 * 2**20),
         name="layer",
     )(
         moe_rows, moe_gain.reshape(1, features), routes.T, route_logit.T,
@@ -645,6 +642,15 @@
         z_in, head_gain.reshape(1, value_rows),
         jnp.swapaxes(w_gate, 1, 2), jnp.swapaxes(w_up, 1, 2), w_down,
     )
+    mixed, moe = pl.pallas_call(
+        emit_kernel,
+        out_shape=(shape((value_rows, length), BF16), shape((tokens, width), BF16)),
+        in_specs=vmem_specs(2),
+        out_specs=tuple([pl.BlockSpec(memory_space=pltpu.HBM)] * 2),
+        scratch_shapes=[dma((2,))],
+        compiler_params=pltpu.CompilerParams(vmem_limit_bytes=8 * 2**20),
+        name="emit",
+    )(mixed, moe)
     return (mixed, moe.T)
 
 

time: 77 us -> 71.1 us (0.923)
  the two profiles are of different devices: /device:TPU:8 before, /device:TPU:4 now
where the time goes in v2:
time: 71.1 us; the launch traced here: 71 us
  Pallas kernels  70.4 us (99%)
    pallas_call x1, Pallas kernels, on_device(): pl.pallas_call(functools.partial(layer_kernel, ep_size=ep_size, tp_size=t...  69.7 us

profile of v2, /device:TPU:4, one launch (start us, length us, event | category | flops | bytes accessed | tf_op | source)
XLA Modules:
  0.0 71.0 jit_solution(13719571267676013192)
XLA Ops:
  0.6 69.7 %layer.1 = (bf16[256,384]{1,0:T(8,128)(2,1)S(1)}, bf16[160,128]{1,0:T(8,128)(2,1)S(1)}) custom-call(bf16[160,2048]{1,0:T(8,128)(2,1)} %rows_hbm.1, f32[1,2048]{1,0:T(1,128)} %bitcast.13, s32[2,160]{1,0:T(2,128)} %bitcast.17, f32[2,160]{1,0:T(2,128)} %bitcast.18, bf16[256,384]{1,0:T(8,128)(2,1)} %x_hbm.1, f32[4,256]{1,0:T(4,128)} %bitcast.14, ...), custom_call_target="tpu_custom_call" | custom-call | tf_op jit(solution)/shard_map/layer/pallas_call | solution.py:604
  70.3 0.7 emit.1

commit v3 on v2

--- a/solution.py
+++ b/solution.py
@@ -22,16 +22,15 @@
 PACK = 80
 PLAN = (
     ("columns",), ("decays",), ("turn", 0), ("turn", 1), ("turn", 2), ("turn", 3), ("gather_own", 0), ("open_rims",),
-    ("b_stream",), ("c_stream",), ("gather_own", 1), ("end_state", 0), ("end_state", 1), ("end_state", 2),
-    ("end_state", 3), ("gather_step", 0, 0), ("scores",), ("spread_states",), ("local_y", 0), ("local_y", 1),
-    ("local_y", 2), ("gather_own", 2), ("local_y", 3), ("gather_step", 1, 0), ("gather_own", 3),
-    ("gather_step", 0, 1), ("gather_step", 2, 0), ("gather_step", 1, 1), ("gather_step", 3, 0), ("gather_step", 0, 2),
-    ("gather_step", 2, 1), ("row_totals",), ("gather_step", 1, 2), ("gather_step", 3, 1), ("gather_step", 0, 3),
-    ("gather_step", 2, 2), ("ffn", 0), ("gather_step", 1, 3), ("gather_step", 3, 2), ("gather_step", 2, 3),
-    ("ffn", 1), ("gather_step", 3, 3), ("scatter_first", 0), ("ffn", 2), ("ffn", 3), ("scatter_first", 1),
-    ("scatter_step", 0, 1), ("incoming",), ("scatter_first", 2), ("scatter_first", 3), ("scatter_step", 1, 1),
-    ("scatter_step", 0, 2), ("scatter_step", 2, 1), ("scatter_step", 3, 1), ("scatter_step", 1, 2),
-    ("scatter_step", 0, 3), ("close", 0), ("close", 1), ("close", 2), ("scatter_step", 2, 2), ("close", 3),
+    ("gather_own", 1), ("b_stream",), ("c_stream",), ("end_state", 0), ("end_state", 1), ("gather_step", 0, 0),
+    ("end_state", 2), ("end_state", 3), ("scores",), ("gather_own", 2), ("spread_states",), ("local_y", 0),
+    ("local_y", 1), ("gather_own", 3), ("local_y", 2), ("gather_step", 1, 0), ("local_y", 3), ("gather_step", 0, 1),
+    ("gather_step", 2, 0), ("gather_step", 3, 0), ("gather_step", 1, 1), ("gather_step", 0, 3), ("gather_step", 0, 2),
+    ("row_totals",), ("gather_step", 2, 1), ("ffn", 0), ("gather_step", 3, 1), ("gather_step", 1, 3),
+    ("gather_step", 1, 2), ("scatter_first", 0), ("ffn", 1), ("gather_step", 2, 3), ("gather_step", 2, 2),
+    ("gather_step", 3, 3), ("gather_step", 3, 2), ("incoming",), ("scatter_first", 1), ("ffn", 2),
+    ("scatter_step", 0, 2), ("ffn", 3), ("scatter_first", 2), ("scatter_first", 3), ("scatter_step", 1, 2),
+    ("scatter_step", 0, 3), ("close", 0), ("close", 1), ("close", 2), ("close", 3), ("scatter_step", 2, 2),
     ("scatter_step", 3, 2), ("scatter_step", 1, 3), ("scatter_last", 0), ("scatter_step", 2, 3),
     ("scatter_step", 3, 3), ("scatter_last", 1), ("scatter_last", 2), ("scatter_last", 3),
 )
@@ -102,7 +101,7 @@
     hops = [(dz, dx) for dz in range(deep) for dx in range(ROWX)]
     near = sorted(hops, key=lambda h: min(h[0], deep - h[0]) + min(h[1], ROWX - h[1]))
     first, second = near[:GROUPED], near[GROUPED : 2 * GROUPED]
-    return first + near[2 * GROUPED :] + second
+    return first + second + near[3 * GROUPED :] + near[2 * GROUPED : 3 * GROUPED]
 
 
 def layer_kernel(
@@ -115,7 +114,7 @@
     ret_out, returned,
     rim_out, rim_in, xrim, brim, crim, tap_col, tapb_col, tapc_col, gain_col,
     step_ref, cum_ref, col_ref, score_ref, bconv_ref, cconv_ref, xs_ref, y_ref,
-    pre1_out, pre1_in, pre2_out, pre2_in, pre3_out, pre3_in, ex_ref, exr_ref,
+    pre1_out, pre1_in, pre2_out, pre2_in, pre3_out, pre3_in, ex_ref, exr_ref, sum_ref,
     in_sem, box_send, box_recv, rim_send, rim_recv, ag_send, ag_recv, sib_send, sib_recv,
     dd_send, dd_recv, rs_send, rs_recv, ret_send, ret_recv, p1_send, p1_recv, p2_send, p2_recv, p3_send, p3_recv,
     *, ep_size, tp_size,
@@ -135,6 +134,15 @@
     span = GROUPED * capacity
     half = span // 2
     wide = GROUPED * pad
+
+    barrier = pltpu.get_barrier_semaphore()
+    for hop in range(1, ep_size):
+        pl.semaphore_signal(barrier, 1, device_id={"ep": (me + hop) % ep_size}, device_id_type=MESH)
+    around = [((chip + 1) % chips) * 2 + core, ((chip + chips - 1) % chips) * 2 + core]
+    beyond = [((chip + 2) % chips) * 2 + core, ((chip + chips - 2) % chips) * 2 + core]
+    sibling = chip * 2 + 1 - core
+    for other in around + beyond + [sibling]:
+        pl.semaphore_signal(barrier, 1, device_id={"tp": other}, device_id_type=MESH)
 
     loads = {}
 
@@ -165,14 +173,6 @@
     load("down", down_hbm.at[0], down_ref)
     load("z", z_hbm, z_ref)
     load("hgain", hgain_hbm, hgain_ref)
-
-    barrier = pltpu.get_barrier_semaphore()
-    for hop in range(1, ep_size):
-        pl.semaphore_signal(barrier, 1, device_id={"ep": (me + hop) % ep_size}, device_id_type=MESH)
-    around = [((chip + 1) % chips) * 2 + core, ((chip + chips - 1) % chips) * 2 + core]
-    sibling = chip * 2 + 1 - core
-    for other in around + [sibling]:
-        pl.semaphore_signal(barrier, 1, device_id={"tp": other}, device_id_type=MESH)
 
     for name in ("routes", "logit"):
         loads[name].wait()
@@ -198,6 +198,12 @@
     normed = (rows_ref[:, mine].astype(F32) * scale * gain_ref[:, mine]).astype(BF16)
     place = lax.broadcasted_iota(jnp.int32, (pad, tokens), 0).astype(F32)
 
+    def arrived(ref, sem):
+        remote(ref, ref, in_sem.at[0], sem, tp=sibling).wait_recv()
+
+    def gone(ref, sem):
+        remote(ref, ref, sem, in_sem.at[0], tp=sibling).wait_send()
+
     def ahead(j):
         dz, dx = hops[j]
         return ((z + dz) % deep) * ROWX + (x + dx) % ROWX
@@ -207,10 +213,10 @@
         return ((z + deep - dz) % deep) * ROWX + (x + ROWX - dx) % ROWX
 
     def box(j):
-        return remote(outbox.at[j], landed.at[j], box_send.at[j], box_recv.at[j], ep=ahead(j))
+        return remote(outbox.at[j], landed.at[j], box_send.at[0], box_recv.at[j // GROUPED], ep=ahead(j))
 
     def back(j):
-        return remote(ret_out.at[j], returned.at[j], ret_send.at[j], ret_recv.at[j], ep=behind(j))
+        return remote(ret_out.at[j], returned.at[j], ret_send.at[0], ret_recv.at[j // GROUPED], ep=behind(j))
 
     def dispatch(team):
         ones = []
@@ -231,6 +237,10 @@
             else:
                 landed[j] = piece
 
+    def received(ref, team):
+        skip = 1 if team == 0 else 0
+        return ref.at[pl.ds(team * GROUPED + skip, GROUPED - skip)]
+
     def packed(ref, team):
         pieces = [ref[team * GROUPED + slot].astype(F32) for slot in range(GROUPED)]
         return jnp.concatenate(pieces, axis=0).astype(BF16)
@@ -343,8 +353,7 @@
 
     def close(head):
         if head == 0:
-            for dx in range(1, ROWX):
-                pre3(dx).wait_recv()
+            arrived(pre3_in.at[pl.ds(0, ROWX - 1)], p3_recv.at[0])
         rows = slice(head * HEAD_DIM, (head + 1) * HEAD_DIM)
         carried = dot(pre3_in[head], cconv_ref[...], ((1,), (0,)))
         y = y_ref[rows, :] + carried * jnp.exp(cum_ref[head : head + 1, :])
@@ -354,14 +363,14 @@
 
     def pre1(dx):
         head = (x + dx) % ROWX
-        return remote(pre1_out.at[head], pre1_in.at[x], p1_send.at[dx], p1_recv.at[dx], ep=z * ROWX + head)
+        return remote(pre1_out.at[head], pre1_in.at[x], p1_send.at[0], p1_recv.at[0], ep=z * ROWX + head)
 
     def pre2(dz):
         return remote(pre2_out, pre2_in.at[z], p2_send.at[dz], p2_recv.at[dz], ep=((z + dz) % deep) * ROWX + x)
 
     def pre3(dx):
         spot = (x + dx) % ROWX
-        return remote(pre3_out.at[spot], pre3_in.at[x], p3_send.at[dx], p3_recv.at[dx], ep=z * ROWX + spot)
+        return remote(pre3_out.at[spot], pre3_in.at[x], p3_send.at[0], p3_recv.at[0], ep=z * ROWX + spot)
 
     def spread_states():
         for dx in range(1, ROWX):
@@ -369,8 +378,7 @@
         pre1_in[x] = pre1_out[x]
 
     def row_totals():
-        for dx in range(1, ROWX):
-            pre1(dx).wait_recv()
+        arrived(pre1_in.at[pl.ds(0, ROWX - 1)], p1_recv.at[0])
         total = jnp.zeros((HEAD_DIM, NSTATE), F32)
         reach = jnp.ones((1, NSTATE), F32)
         for spot in range(ROWX):
@@ -411,41 +419,39 @@
 
     def ag(d, team, step):
         sign = 1 - 2 * d
-        origin = ((chip + chips - sign * step) % chips) * 2 + core
+        hop = min(step, far - 2)
+        origin = ((chip + chips - sign * hop) % chips) * 2 + core
         start, count = at_rows(team, d, step)
         ref = xall.at[origin, pl.ds(start, count), :]
-        return remote(ref, ref, ag_send.at[d, team, step], ag_recv.at[d, team, step], tp=around[d])
+        target = around[d] if step < far - 1 else beyond[d]
+        return remote(ref, ref, ag_send.at[0], ag_recv.at[team, step], tp=target)
 
     def sib(team, d, step):
         sign = 1 - 2 * d
         origin = ((chip + chips - sign * (step + 1)) % chips) * 2 + core
         start, count = at_rows(team, d, step)
         ref = xall.at[origin, pl.ds(start, count), :]
-        index = 0 if step < 0 else 1 + d * far + step
-        return remote(ref, ref, sib_send.at[team, index], sib_recv.at[team, index], tp=sibling)
-
-    def arrivals():
-        return [(0, -1)] + [(d, step) for step in range(far) for d in range(2)]
+        return remote(ref, ref, sib_send.at[0], sib_recv.at[team], tp=sibling)
 
     def gather_own(team):
-        for slot in range(GROUPED):
-            if team or slot:
-                box(team * GROUPED + slot).wait_recv()
+        arrived(received(landed, team), box_recv.at[team])
         xall[lane, team * span : (team + 1) * span, :] = packed(landed, team)
         for d in range(2):
             ag(d, team, 0).start()
         sib(team, 0, -1).start()
 
     def gather_step(team, step):
+        arrived(xall.at[0, pl.ds(0, 2 * at_rows(team, 0, step)[1]), :], ag_recv.at[team, step])
         for d in range(2):
-            ag(d, team, step).wait_recv()
-            if step + 1 < far:
+            if step + 1 < far - 1:
                 ag(d, team, step + 1).start()
+        for d in range(2):
+            if step == far - 3:
+                ag(d, team, far - 1).start()
             sib(team, d, step).start()
 
     def ffn(team):
-        for d, step in arrivals():
-            sib(team, d, step).wait_recv()
+        arrived(xall.at[pl.ds(0, chips // teams)], sib_recv.at[team])
         rows = slice(team * span, (team + 1) * span)
         tokens_in = jnp.concatenate([xall[i, rows, :] for i in range(tp_size)], axis=1)
         both = dot(tokens_in, gut_ref[...], ((1,), (0,)))
@@ -455,19 +461,10 @@
         out = dot(jnp.concatenate([hidden, extra], axis=1), down_ref[...], ((1,), (0,)))
         for i in range(tp_size):
             part[team, i % 2, i // 2] = out[:, i * width : (i + 1) * width].astype(BF16)
-        for reach in order_of_need:
-            cross(team, reach).start()
-
-    order_of_need = [far]
-    for away in range(far - 1, 0, -1):
-        order_of_need += [away, chips - away]
-    order_of_need.append(0)
-
-    def cross(team, reach):
-        at = (chip + reach) % chips
-        return remote(
-            part.at[team, 1 - core, at], sibp.at[team, at], dd_send.at[team, reach], dd_recv.at[team, reach], tp=sibling
-        )
+        cross(team).start()
+
+    def cross(team):
+        return remote(part.at[team, 1 - core], sibp.at[team], dd_send.at[0], dd_recv.at[team], tp=sibling)
 
     def own_sum(team, reach):
         at = (chip + reach) % chips
@@ -477,11 +474,17 @@
         start, count = (d * half, half) if step == 0 else (0, span)
         return remote(
             rs_out.at[d, team, step, pl.ds(start, count), :], rs_in.at[d, team, step, pl.ds(start, count), :],
-            rs_send.at[d, team, step], rs_recv.at[d, team, step], tp=around[d],
+            rs_send.at[0], rs_recv.at[team, max(step - 1, 0)], tp=around[d] if step else beyond[d],
         )
 
+    def reach_of(d, away):
+        return away if d == 0 else chips - away
+
     def scatter_first(team):
-        cross(team, far).wait_recv()
+        cross(team).wait_recv()
+        for d in range(2):
+            rs_out[d, team, 1] = own_sum(team, reach_of(d, far - 1)).astype(BF16)
+            rs(d, team, 1).start()
         total = own_sum(team, far).astype(BF16)
         for d in range(2):
             cut = slice(d * half, (d + 1) * half)
@@ -489,25 +492,23 @@
             rs(d, team, 0).start()
 
     def scatter_step(team, step):
+        count = 3 * span if step == 2 else 2 * span
+        arrived(xall.at[0, pl.ds(0, count), :], rs_recv.at[team, step - 2])
         for d in range(2):
-            reach = far - step if d == 0 else chips - (far - step)
-            cross(team, reach).wait_recv()
-            total = own_sum(team, reach)
-            rs(d, team, step - 1).wait_recv()
-            if step == 1:
+            total = own_sum(team, reach_of(d, far - step)) + rs_in[d, team, step - 1].astype(F32)
+            if step == 2:
                 cut = slice(d * half, (d + 1) * half)
                 other = slice((1 - d) * half, (2 - d) * half)
                 rs_out[d, team, step, other, :] = total[other].astype(BF16)
                 rs_out[d, team, step, cut, :] = (total[cut] + rs_in[d, team, 0, cut, :].astype(F32)).astype(BF16)
             else:
-                rs_out[d, team, step] = (total + rs_in[d, team, step - 1].astype(F32)).astype(BF16)
+                rs_out[d, team, step] = total.astype(BF16)
             rs(d, team, step).start()
 
     def scatter_last(team):
-        cross(team, 0).wait_recv()
         total = own_sum(team, 0)
+        arrived(xall.at[0, pl.ds(0, 2 * span), :], rs_recv.at[team, far - 2])
         for d in range(2):
-            rs(d, team, far - 1).wait_recv()
             total = total + rs_in[d, team, far - 1].astype(F32)
         for slot in range(GROUPED):
             j = team * GROUPED + slot
@@ -518,8 +519,8 @@
             else:
                 returned[j] = piece
 
-    pl.semaphore_wait(barrier, ep_size - 1 + len(around) + 1)
-    for team in (0, 2, 1, 3):
+    pl.semaphore_wait(barrier, ep_size - 1 + len(around) + len(beyond) + 1)
+    for team in range(teams):
         dispatch(team)
     send_rims()
     parts = (
@@ -529,43 +530,37 @@
     named = {part.__name__: part for part in parts}
     for step in PLAN:
         named[step[0]](*step[1:])
-    def combine():
-        total = jnp.zeros((tokens, width), F32)
-        for team in range(teams):
-            for slot in range(GROUPED):
-                if team or slot:
-                    back(team * GROUPED + slot).wait_recv()
-            total = total + dot(pick_ref[team * wide : (team + 1) * wide, :], packed(returned, team), ((0,), (0,)))
-        moe_ref[...] = total.astype(BF16)
-
-    combine()
-
-    for j in range(1, ep_size):
-        box(j).wait_send()
-        back(j).wait_send()
+    def combine(team):
+        arrived(received(returned, team), ret_recv.at[team])
+        now = dot(pick_ref[team * wide : (team + 1) * wide, :], packed(returned, team), ((0,), (0,)))
+        if team == 0:
+            sum_ref[...] = now
+        elif team + 1 < teams:
+            sum_ref[...] = sum_ref[...] + now
+        else:
+            moe_ref[...] = (sum_ref[...] + now).astype(BF16)
+
+    for team in range(teams):
+        combine(team)
+
+    gone(outbox.at[pl.ds(1, ep_size - 1)], box_send.at[0])
+    gone(ret_out.at[pl.ds(1, ep_size - 1)], ret_send.at[0])
+    gone(xall.at[pl.ds(0, chips - 1)], ag_send.at[0])
+    gone(xall.at[pl.ds(0, chips - 1)], rs_send.at[0])
+    gone(xall.at[pl.ds(0, chips)], sib_send.at[0])
+    gone(xall.at[pl.ds(0, chips)], dd_send.at[0])
+    gone(pre1_out.at[pl.ds(0, ROWX - 1)], p1_send.at[0])
+    gone(pre3_out.at[pl.ds(0, ROWX - 1)], p3_send.at[0])
 
     @pl.when(me + 1 < ep_size)
     def _():
         rim.wait_send()
 
-    for dx in range(1, ROWX):
-        pre1(dx).wait_send()
-        pre3(dx).wait_send()
     for dz in range(1, deep):
 
         @pl.when(z + dz < deep)
         def _(dz=dz):
             pre2(dz).wait_send()
-
-    for team in range(teams):
-        for d in range(2):
-            for step in range(far):
-                ag(d, team, step).wait_send()
-                rs(d, team, step).wait_send()
-        for d, step in arrivals():
-            sib(team, d, step).wait_send()
-        for reach in range(chips):
-            cross(team, reach).wait_send()
 
 
 def emit_kernel(mixed_ref, moe_ref, mixed_out, moe_out, sems):
@@ -628,11 +623,11 @@
             VMEM((heads, PACK, NSTATE), BF16), VMEM((ROWX, PACK, NSTATE), BF16),
             VMEM((PACK, NSTATE), BF16), VMEM((deep, PACK, NSTATE), BF16),
             VMEM((ROWX, HEAD_DIM, NSTATE), BF16), VMEM((ROWX, HEAD_DIM, NSTATE), BF16),
-            VMEM((ROWX, HEAD_DIM, NSTATE), F32), VMEM((ROWX, 8, NSTATE), F32),
-            dma((19,)), dma((ep_size,)), dma((ep_size,)), dma((1,)), dma((1,)),
-            dma((2, teams, far)), dma((2, teams, far)), dma((teams, 1 + 2 * far)), dma((teams, 1 + 2 * far)),
-            dma((teams, chips)), dma((teams, chips)), dma((2, teams, far)), dma((2, teams, far)),
-            dma((ep_size,)), dma((ep_size,)), dma((ROWX,)), dma((ROWX,)), dma((deep,)), dma((deep,)), dma((ROWX,)), dma((ROWX,)),
+            VMEM((ROWX, HEAD_DIM, NSTATE), F32), VMEM((ROWX, 8, NSTATE), F32), VMEM((tokens, width), F32),
+            dma((19,)), dma((1,)), dma((teams,)), dma((1,)), dma((1,)),
+            dma((1,)), dma((teams, far)), dma((1,)), dma((teams,)),
+            dma((1,)), dma((teams,)), dma((1,)), dma((teams, far - 1)),
+            dma((1,)), dma((teams,)), dma((1,)), dma((1,)), dma((deep,)), dma((deep,)), dma((1,)), dma((1,)),
         ],
         compiler_params=pltpu.CompilerParams(collective_id=0, has_side_effects=True, vmem_limit_bytes=60 * 2**20),
         name="layer",

time: 71.1 us -> 65 us (0.914)
  the two profiles are of different devices: /device:TPU:4 before, /device:TPU:8 now
where the time goes in v3:
time: 65 us; the launch traced here: 64.8 us
  Pallas kernels  64.2 us (99%)
  between operations  0.65 us (1%)
    pallas_call x1, Pallas kernels, on_device(): pl.pallas_call(functools.partial(layer_kernel, ep_size=ep_size, tp_size=t...  63.5 us

profile of v3, /device:TPU:8, one launch (start us, length us, event | category | flops | bytes accessed | tf_op | source)
XLA Modules:
  0.0 64.8 jit_solution(15999177532485319305)
XLA Ops:
  0.6 63.5 %layer.1 = (bf16[256,384]{1,0:T(8,128)(2,1)S(1)}, bf16[160,128]{1,0:T(8,128)(2,1)S(1)}) custom-call(bf16[160,2048]{1,0:T(8,128)(2,1)} %rows_hbm.1, f32[1,2048]{1,0:T(1,128)} %bitcast.13, s32[2,160]{1,0:T(2,128)} %bitcast.17, f32[2,160]{1,0:T(2,128)} %bitcast.18, bf16[256,384]{1,0:T(8,128)(2,1)} %x_hbm.1, f32[4,256]{1,0:T(4,128)} %bitcast.14, ...), custom_call_target="tpu_custom_call" | custom-call | tf_op jit(solution)/shard_map/layer/pallas_call | solution.py:599
  64.1 0.7 %emit.1 = (bf16[256,384]{1,0:T(8,128)(2,1)}, bf16[160,128]{1,0:T(8,128)(2,1)}) custom-call(bf16[256,384]{1,0:T(8,128)(2,1)S(1)} %get-tuple-element.6.mixed_ref, bf16[160,128]{1,0:T(8,128)(2,1)S(1)} %get-tuple-element.7.moe_ref), custom_call_target="tpu_custom_call" | custom-call | tf_op jit(solution)/shard_map/emit/pallas_call | solution.py:640
